TPU v7x, 128 devices: a 2x2x16 block of a 8x8x16 slice. The times are simulated.
128 devices in a mesh: grp: 4 (over y, x), ep: 32 (over z, core).
Axes of the slice: x: 2, y: 2, z: 16, core: 2. Of those that a mesh axis runs over, the one named last changes fastest.
The devices are a block of a 8x8x16 slice.
Arguments:
- tokens: bfloat16 [32768, 2048], P(('grp', 'ep')), parts along dimension 0, may hold values from -6 to 6
- norm_gain: float32 [2048], replicated, may hold values from 0.1 to 1.9
- expert_ids: int32 [32768, 2], P(('grp', 'ep')), parts along dimension 0, may hold values from 0 to 31, all different within a row; in each aligned block of 256 rows (0 to 255, 256 to 511, ...) at most 32 rows name the same one
- gate_weights: float32 [32768, 2], P(('grp', 'ep')), parts along dimension 0, may hold values from 0.1 to 1
- w_gate: bfloat16 [32, 2048, 1024], P('ep'), may hold values from -0.125 to 0.125
- w_up: bfloat16 [32, 2048, 1024], P('ep'), may hold values from -0.125 to 0.125
- w_down: bfloat16 [32, 1024, 2048], P('ep'), may hold values from -0.1875 to 0.1875
Outputs:
- mixed: bfloat16 [32768, 2048], P(('grp', 'ep')), parts along dimension 0
There are 4 independent parts, one for each index of `grp`. A program takes and returns all parts, laid end to end along the dimension named above; an argument that names none is the same for every part. Nothing has to cross between parts.
Inputs may be any that keep to these rules, and one draw needn't show every extreme that they name: `expert_ids`: A token's 2 experts are distinct. Within the rows of one device (aligned blocks of 256 tokens) no expert is named more than 32 times, and in some block one expert is named exactly 32 times.
All inputs are finite; a program needn't handle non-finite values.
Results may differ from a plain program's by a relative error of at most 0.0071.
Values may be sent and summed in bfloat16 or wider, within the bound.
No kernel may reach another device: no remote copies, remote signals or barrier semaphores. Data moves between devices by JAX's collectives and lax.ppermute only.
A program may use at most 64 MiB of HBM per device.

v0:
```python
import jax
import jax.numpy as jnp
from jax import lax
from jax.sharding import PartitionSpec as P


def per_device(tokens, norm_gain, expert_ids, gate_weights, w_gate, w_up, w_down):
    experts = lax.axis_size("ep")
    tok_rows, feature_width = tokens.shape
    top_count = expert_ids.shape[1]
    capacity = 2 * tok_rows * top_count // experts
    values = tokens.astype(jnp.float32)
    normed = (
        values * lax.rsqrt(jnp.mean(values * values, -1, keepdims=True) + 1e-06) * norm_gain
    ).astype(jnp.bfloat16)
    flat_ids = expert_ids.reshape(-1)
    onehot = (flat_ids[:, None] == jnp.arange(experts, dtype=jnp.int32)[None, :]).astype(jnp.int32)
    before = jnp.cumsum(onehot, axis=0) - onehot
    slots = jnp.sum(onehot * before, axis=1)
    dest = flat_ids * capacity + slots
    copies = jnp.repeat(normed, top_count, axis=0)
    outgoing = jnp.zeros((experts * capacity, feature_width), jnp.bfloat16).at[dest].set(copies)
    outgoing = outgoing.reshape(experts, capacity, feature_width)
    arrived = lax.all_to_all(outgoing, "ep", split_axis=0, concat_axis=0, tiled=True)
    rows = arrived.reshape(-1, feature_width)
    gate = jnp.dot(rows, w_gate[0], preferred_element_type=jnp.float32)
    upper = jnp.dot(rows, w_up[0], preferred_element_type=jnp.float32)
    hidden = (jax.nn.silu(gate) * upper).astype(jnp.bfloat16)
    result = jnp.dot(hidden, w_down[0], preferred_element_type=jnp.float32).astype(jnp.bfloat16)
    finished = result.reshape(arrived.shape)
    returned = lax.all_to_all(finished, "ep", split_axis=0, concat_axis=0, tiled=True)
    returned = returned.reshape(experts * capacity, feature_width)
    back = returned[dest].astype(jnp.float32).reshape(tok_rows, top_count, feature_width)
    mixed = jnp.sum(back * gate_weights[:, :, None], axis=1)
    return mixed.astype(jnp.bfloat16)


def solution(mesh):
    return jax.shard_map(
        per_device,
        mesh=mesh,
        in_specs=(
            P(("grp", "ep"), None),
            P(),
            P(("grp", "ep"), None),
            P(("grp", "ep"), None),
            P("ep", None, None),
            P("ep", None, None),
            P("ep", None, None),
        ),
        out_specs=P(("grp", "ep"), None),
        check_vma=False,
    )
```

profile of v0, /device:TPU:86, one launch (start us, length us, event | category | flops | bytes accessed | tf_op | source)
XLA Modules:
  0.0 459.1 jit_solution(10212200483092486496)
XLA Ops:
  0.0 0.8 copy.10
  0.8 0.1 eq.29
  1.0 0.1 eq.25
  1.1 0.7 broadcast_multiply_fusion
  1.8 1.2 reduce-window.6
  3.0 0.2 slice_reduce_fusion
  3.2 0.1 copy.9
  3.4 0.1 mul.55
  3.5 1.5 fusion.11
  5.1 1.5 fusion.13
  6.6 1.3 broadcast_in_dim.5
  7.9 2.2 reshape.94
  10.1 0.1 fusion.18
  10.2 7.2 %scatter_custom_fusion = bf16[1024,2048]{1,0:T(8,128)(2,1)} fusion(s32[512]{0:T(512)S(1)} %bitcast.45, bf16[512,2048]{1,0:T(8,128)(2,1)} %reshape.94, bf16[]{:T(256)} %constant.8.clone.1), kind=kCustom, calls=%fused_computation.16 | custom fusion | bytes 4194816 | tf_op jit(solution)/shard_map/scatter | solution.py:22
  17.4 0.0 copy-start.1
  17.4 208.2 %all_to_all.10 = bf16[32,32,2048]{2,1,0:T(8,128)(2,1)S(1)} all-to-all(bf16[32,32,2048]{2,1,0:T(8,128)(2,1)} %bitcast.41), channel_id=1, replica_groups=mesh['grp'=4,'ep'=32] {'ep'}, dimensions={0} | all-to-all | bytes 8388608 | tf_op jit(solution)/shard_map/all_to_all | solution.py:24
  225.6 0.0 copy-done.1
  225.6 0.0 copy-start.2
  225.6 4.5 fusion.2
  230.2 0.0 copy-done.2
  230.2 0.0 copy-start.3
  230.2 5.4 %multiply_convert_fusion = bf16[1024,1024]{1,0:T(8,128)(2,1)S(1)} fusion(f32[1024,1024]{1,0:T(8,128)S(1)} %fusion.2, bf16[1024,2048]{1,0:T(8,128)(2,1)S(1)} %bitcast.44, bf16[1,2048,1024]{2,1,0:T(8,128)(2,1)S(1)} %copy-done.2), kind=kOutput, calls=%fused_computation.9 | convolution fusion | flops 4301258752 | bytes 14680064 | tf_op jit(solution)/shard_map/dot_general | solution.py:26
  235.6 0.0 copy-done.3
  235.6 6.1 %fusion.6 = bf16[1024,2048]{1,0:T(8,128)(2,1)} fusion(bf16[1024,1024]{1,0:T(8,128)(2,1)S(1)} %multiply_convert_fusion, bf16[1,1024,2048]{2,1,0:T(8,128)(2,1)S(1)} %copy-done.3), kind=kOutput, calls=%fused_computation.10 | convolution fusion | flops 4297064448 | bytes 10485760 | tf_op jit(solution)/shard_map/dot_general | solution.py:29
  241.7 0.0 copy-start
  241.7 6.0 %all-to-all-start.1 = ((bf16[32,32,2048]{2,1,0:T(8,128)(2,1)}), bf16[32,32,2048]{2,1,0:T(8,128)(2,1)}, u32[]{:S(2)}, u32[]{:S(2)}) async-start(bf16[32,32,2048]{2,1,0:T(8,128)(2,1)} %bitcast.42), calls=%async_computation.1 | async-start | bytes 8388608 | tf_op jit(solution)/shard_map/all_to_all | solution.py:31
  247.7 0.0 copy-done
  247.7 0.1 copy.13
  247.8 190.2 %all-to-all-done.1 = bf16[32,32,2048]{2,1,0:T(8,128)(2,1)} async-done(((bf16[32,32,2048]{2,1,0:T(8,128)(2,1)}), bf16[32,32,2048]{2,1,0:T(8,128)(2,1)}, u32[]{:S(2)}, u32[]{:S(2)}) %all-to-all-start.1) | async-done | bytes 4194336 | tf_op jit(solution)/shard_map/all_to_all | solution.py:31
  438.1 7.1 %gather_fusion = bf16[512,2048]{1,0:T(8,128)(2,1)S(1)} fusion(bf16[1024,2048]{1,0:T(8,128)(2,1)} %bitcast.9, s32[1024]{0:T(1024)S(1)} %pad_clamp_fusion), kind=kCustom, calls=%fused_computation | custom fusion | bytes 4196352 | tf_op jit(solution)/shard_map/gather | solution.py:33
  445.2 4.0 reshape.81
  449.2 9.9 %multiply_reduce_fusion = bf16[256,2048]{1,0:T(8,128)(2,1)} fusion(f32[256,2,2048]{2,1,0:T(2,128)} %reshape.81, f32[256,2]{1,0:T(8,128)S(1)} %copy.13), kind=kLoop, calls=%fused_computation.8 | loop fusion | flops 1572864 | bytes 5244928 | tf_op jit(solution)/shard_map/reduce_sum | solution.py:34
  (6 shorter events, 0.1 us)
Async XLA Ops:
  17.4 208.2 %copy-start.1 = (bf16[1,2048,1024]{2,1,0:T(8,128)(2,1)S(1)}, bf16[1,2048,1024]{2,1,0:T(8,128)(2,1)}, u32[]{:S(2)}) copy-start(bf16[1,2048,1024]{2,1,0:T(8,128)(2,1)} %param.12) | copy-start | bytes 12582916
  225.6 4.5 copy-start.2
  230.2 5.4 %copy-start.3 = (bf16[1,1024,2048]{2,1,0:T(8,128)(2,1)S(1)}, bf16[1,1024,2048]{2,1,0:T(8,128)(2,1)}, u32[]{:S(2)}) copy-start(bf16[1,1024,2048]{2,1,0:T(8,128)(2,1)} %param.13) | copy-start | bytes 12582916
  241.7 6.0 %copy-start = (f32[256,2]{0,1:T(2,128)S(1)}, f32[256,2]{0,1:T(2,128)}, u32[]{:S(2)}) copy-start(f32[256,2]{0,1:T(2,128)} %param.10) | copy-start | bytes 6148
  241.7 196.4 %all-to-all-start.1 = ((bf16[32,32,2048]{2,1,0:T(8,128)(2,1)}), bf16[32,32,2048]{2,1,0:T(8,128)(2,1)}, u32[]{:S(2)}, u32[]{:S(2)}) async-start(bf16[32,32,2048]{2,1,0:T(8,128)(2,1)} %bitcast.42), calls=%async_computation.1 | async-start | bytes 8388608 | tf_op jit(solution)/shard_map/all_to_all | solution.py:31
where the time goes:
time: 459 us
  blocking collectives  208 us (45%)
  waiting for transfers between devices  190 us (41%)
  local copies, waits for them, and re-layouts  23.6 us (5%)
  matrix products  16 us (3%)
  other arithmetic  14.9 us (3%)
  starting transfers between devices  6 us (1%)
    all_to_all x1, blocking collectives, per_device(): lax.all_to_all(outgoing, 'ep', split_axis=0, concat_axis=0, tiled=True)  208 us
    all_to_all x1, waiting for transfers between devices, per_device(): lax.all_to_all(finished, 'ep', split_axis=0, concat_axis=0, tiled=True)  190 us
    reduce_sum x1, other arithmetic, per_device(): mixed = jnp.sum(back * gate_weights[:, :, None], axis=1)  9.86 us
  transfers between devices with their start and end apart: 1, of which 1 were waited for; matrix products, arithmetic and copies ran while one was open for 0% of the time, Pallas kernels for 0%

commit v1 on v0

v1 whole, which is shorter than its diff:
```python
import jax
import jax.numpy as jnp
from jax import lax
from jax.sharding import PartitionSpec as P

BF = jnp.bfloat16
F32 = jnp.float32
HALVES = 2


def dot(a, b, dims=((1,), (0,))):
    return lax.dot_general(a, b, (dims, ((), ())), preferred_element_type=F32)


def per_device(tokens, norm_gain, expert_ids, gate_weights, w_gate, w_up, w_down):
    ep = lax.axis_size("ep")
    chips = ep // 2
    far = chips // 2
    rows, width = tokens.shape
    cap = 2 * rows * expert_ids.shape[1] // ep
    size = {t: min(rows, cap * (2 * (far - t) + 1)) for t in range(1, far + 1)}
    near = max(t for t in size if size[t] == rows)
    part = width // HALVES
    me = lax.axis_index("ep")
    chip, core = me // 2, me % 2

    def shift(x, hops):
        return lax.ppermute(x, "ep", [(i, (i + 2 * hops) % ep) for i in range(ep)])

    def swap(x):
        return lax.ppermute(x, "ep", [(i, i ^ 1) for i in range(ep)])

    values = tokens.astype(F32)
    scale = lax.rsqrt(jnp.mean(values * values, -1) + 1e-06)
    code = (expert_ids[:, 0] * ep + expert_ids[:, 1]).astype(F32)
    meta = jnp.stack([code, gate_weights[:, 0], gate_weights[:, 1], scale])
    order = [0]
    for t in range(1, far):
        order += [t, -t]
    order.append(far)
    where = {d: i for i, d in enumerate(order)}
    metas = jnp.stack([meta if d == 0 else shift(meta, d) for d in order])
    codes = metas[:, 0].astype(jnp.int32)
    first, second = codes // ep, codes % ep
    experts = jnp.stack([me, me ^ 1])[None, :, None]
    hit1 = first[:, None, :] == experts
    hit2 = second[:, None, :] == experts
    hit = hit1 | hit2
    weight = jnp.where(hit1, metas[:, None, 1], 0.0) + jnp.where(hit2, metas[:, None, 2], 0.0)
    before = (
        lax.broadcasted_iota(jnp.int32, (rows, rows), 0)
        < lax.broadcasted_iota(jnp.int32, (rows, rows), 1)
    ).astype(BF)
    slot = dot(hit.astype(BF).reshape(-1, rows), before).reshape(hit.shape)
    picks = hit[:, :, None, :] & (
        slot[:, :, None, :] == jnp.arange(cap, dtype=F32)[None, None, :, None]
    )
    high = lax.reduce_precision(weight, 8, 7)
    low = weight - high

    def spread(v):
        return jnp.where(picks, v, 0.0).astype(BF).reshape(chips, 2 * cap, rows)

    pick = picks.astype(BF).reshape(chips, 2 * cap, rows)
    pick_high = spread(high[:, :, None, :])
    pick_low = spread(low[:, :, None, :])
    row_scale = jnp.sum(jnp.where(picks, metas[:, 3][:, None, None, :], 0.0), -1).reshape(
        chips, 2 * cap
    )
    edge_weight = jnp.sum(jnp.where(picks[-1], weight[-1][:, None, :], 0.0), -1)

    def ordering(d, way):
        source = (chip - d) % chips
        best = jnp.zeros((rows,), jnp.int32)
        for ids in (first[where[d]], second[where[d]]):
            dist = (way * (ids // 2 - source)) % chips
            good = (dist < far) | ((dist == far) & (ids % 2 == (0 if way == 1 else 1)))
            best = jnp.maximum(best, jnp.where(good, dist, 0))
        return best

    combos = [(t if t == far else way * t, way) for t in range(near, far) for way in (1, -1)]
    reach = jnp.stack([ordering(d, way) for d, way in combos])
    levels = jnp.arange(far, near, -1, dtype=jnp.int32)
    at = reach[:, None, :] == levels[None, :, None]
    rank_in = dot(at.astype(BF).reshape(-1, rows), before).reshape(at.shape)
    total = jnp.sum(at.astype(F32), -1)
    base = jnp.cumsum(total, 1) - total
    rank = jnp.sum(jnp.where(at, rank_in + base[:, :, None], 0.0), 1)
    rank = jnp.where(reach > near, rank, -1.0)
    place = (
        rank[:, None, :] == jnp.arange(size[near + 1], dtype=F32)[None, :, None]
    ).astype(BF)

    pieces = [tokens[:, h * part : (h + 1) * part] for h in range(HALVES)]
    gains = [norm_gain[h * part : (h + 1) * part] for h in range(HALVES)]

    def chosen(select, packet, d):
        return [
            (dot(select, packet[h]) * row_scale[where[d]][:, None] * gains[h]).astype(BF)
            for h in range(HALVES)
        ]

    def sorted_picks(t, way):
        i = combos.index((way * t, way))
        w = where[way * t]
        three = jnp.concatenate([pick[w], pick_high[w], pick_low[w]], 0)
        return dot(three, place[i][: size[t]], ((1,), (1,))).astype(BF)

    packet = {1: pieces, -1: pieces}
    picked = {0: [chosen(pick[0], pieces, 0)]}
    backs = {}
    for t in range(1, far + 1):
        for way in (1, -1):
            if t == near + 1:
                i = combos.index((way * near, way))
                packet[way] = [dot(place[i], p).astype(BF) for p in packet[way]]
            packet[way] = [shift(p[: size[t]], way) for p in packet[way]]
        if t < far:
            for way in (1, -1):
                w = where[way * t]
                if t <= near:
                    select = pick[w]
                    backs[t, way] = jnp.concatenate([pick_high[w], pick_low[w]], 0)
                else:
                    three = sorted_picks(t, way)
                    select = three[: 2 * cap]
                    backs[t, way] = three[2 * cap :]
                picked.setdefault(t, []).append(chosen(select, packet[way], way * t))
        else:
            sides = []
            for which in (0, 1):
                s = row_scale[-1][which * cap : (which + 1) * cap, None]
                sides.append(
                    [
                        (
                            jnp.where(core == which, packet[1][h], packet[-1][h]).astype(F32)
                            * s
                            * gains[h]
                        ).astype(BF)
                        for h in range(HALVES)
                    ]
                )
            picked[t] = [[jnp.concatenate([sides[0][h], sides[1][h]], 0) for h in range(HALVES)]]

    groups = [[0, 1, 2], [3, 4], [5, 6], [far - 1, far]]
    done = {}
    for group in groups:
        blocks = [(t, j) for t in group for j in range(len(picked[t]))]
        full = [jnp.concatenate(picked[t][j], 1) for t, j in blocks]
        own = jnp.concatenate([b[:cap] for b in full], 0)
        other = jnp.concatenate([b[cap:] for b in full], 0)
        x = jnp.concatenate([own, swap(other)], 0)
        gate = dot(x, w_gate[0])
        upper = dot(x, w_up[0])
        hidden = (jax.nn.silu(gate) * upper).astype(BF)
        result = dot(hidden, w_down[0]).astype(BF)
        n = len(blocks) * cap
        theirs = swap(result[n:])
        for k, key in enumerate(blocks):
            s = slice(k * cap, (k + 1) * cap)
            done[key] = (result[s], theirs[s])

    def twice(key, h):
        both = jnp.concatenate(done[key], 0)[:, h * part : (h + 1) * part]
        return jnp.concatenate([both, both], 0)

    coming = {1: None, -1: None}
    mine, theirs = done[far, 0]
    mine = (mine.astype(F32) * edge_weight[0][:, None]).astype(BF)
    theirs = (theirs.astype(F32) * edge_weight[1][:, None]).astype(BF)
    for way in (1, -1):
        side = jnp.where(core == (0 if way == 1 else 1), mine, theirs)
        coming[way] = [shift(side[:, h * part : (h + 1) * part], -way) for h in range(HALVES)]
    for t in range(far - 1, 0, -1):
        for way in (1, -1):
            sums = []
            for h in range(HALVES):
                add = dot(backs[t, way], twice((t, 0 if way == 1 else 1), h), ((0,), (0,)))
                got = coming[way][h]
                if t == near:
                    i = combos.index((way * near, way))
                    add = add + dot(place[i], got, ((0,), (0,)))
                else:
                    got = got.astype(F32)
                    add = add + jnp.pad(got, ((0, size[t] - got.shape[0]), (0, 0)))
                sums.append(shift(add.astype(BF), -way))
            coming[way] = sums
    outs = []
    back = jnp.concatenate([pick_high[0], pick_low[0]], 0)
    for h in range(HALVES):
        total = dot(back, twice((0, 0), h), ((0,), (0,)))
        total = total + coming[1][h].astype(F32) + coming[-1][h].astype(F32)
        outs.append(total.astype(BF))
    return jnp.concatenate(outs, 1)


def solution(mesh):
    return jax.shard_map(
        per_device,
        mesh=mesh,
        in_specs=(
            P(("grp", "ep"), None),
            P(),
            P(("grp", "ep"), None),
            P(("grp", "ep"), None),
            P("ep", None, None),
            P("ep", None, None),
            P("ep", None, None),
        ),
        out_specs=P(("grp", "ep"), None),
        check_vma=False,
    )
```

time: 459 us -> 422 us (0.919); the launches traced: 459 us -> 415 us
  blocking collectives: 208 us -> 0 us
  starting transfers between devices: 6 us -> 169 us
  waiting for transfers between devices: 190 us -> 131 us
  matrix products: 16 us -> 71.2 us
    all_to_all x1 -> x0, blocking collectives: 208 us -> none  [per_device(): lax.all_to_all(outgoing, 'ep', split_axis=0, concat_axis=0, tiled=True)]
    all_to_all x1 -> x0, waiting for transfers between devices: 190 us -> none  [per_device(): lax.all_to_all(finished, 'ep', split_axis=0, concat_axis=0, tiled=True)]
    ppermute x0 -> x87, starting transfers between devices: none -> 169 us  [the longest x79 167 us: shift(): return lax.ppermute(x, 'ep', [(i, (i + 2 * hops) % ep) for i in range(ep)])]
    ppermute x0 -> x87, waiting for transfers between devices: none -> 131 us  [the longest x79 131 us: shift(): return lax.ppermute(x, 'ep', [(i, (i + 2 * hops) % ep) for i in range(ep)])]
    dot_general x3 -> x84, matrix products: 16 us -> 71.2 us  [dot(): return lax.dot_general(a, b, (dims, ((), ())), preferred_element_type=F32)]
    slice x1 -> x33, local copies, waits for them, and re-layouts: 0.22 us -> 14.7 us  [the longest x6 4.48 us: per_device(): done[key] = (result[s], theirs[s])]
    reduce_sum x3 -> x4, other arithmetic: 11.5 us -> 2.09 us  [the longest x1 1.52 us: per_device(): scale = lax.rsqrt(jnp.mean(values * values, -1) + 1e-06)]
    concatenate x0 -> x21, other arithmetic: none -> 7.72 us  [the longest x13 4.44 us: twice(): both = jnp.concatenate(done[key], 0)[:, h * part:(h + 1) * part]]
  transfers between devices with their start and end apart: 1 -> 87, of which waited for: 1 -> 27; matrix products, arithmetic and copies ran while one was open for 0% -> 25% of each run, Pallas kernels for 0% -> 0%
where the time goes in v1:
time: 422 us; the launch traced here: 415 us
  starting transfers between devices  169 us (40%)
  waiting for transfers between devices  131 us (31%)
  matrix products  71.2 us (17%)
  local copies, waits for them, and re-layouts  25.2 us (6%)
  other arithmetic  16.4 us (4%)
    ppermute x79, starting transfers between devices, shift(): return lax.ppermute(x, 'ep', [(i, (i + 2 * hops) % ep) for i in range(ep)])  167 us
    ppermute x79, waiting for transfers between devices, shift(): return lax.ppermute(x, 'ep', [(i, (i + 2 * hops) % ep) for i in range(ep)])  131 us
    dot_general x84, matrix products, dot(): return lax.dot_general(a, b, (dims, ((), ())), preferred_element_type=F32)  71.2 us
  transfers between devices with their start and end apart: 87, of which 27 were waited for; matrix products, arithmetic and copies ran while one was open for 25% of the time, Pallas kernels for 0%

profile of v1, /device:TPU:86, one launch (start us, length us, event | category | flops | bytes accessed | tf_op | source)
XLA Modules:
  0.0 414.8 jit_solution(1643390873493795726)
XLA Ops:
  3.1 15.3 %collective-permute-start.13 = (f32[4,256]{1,0:T(4,128)S(1)}, f32[4,256]{1,0:T(4,128)S(1)}, u32[]{:S(2)}, u32[]{:S(2)}) collective-permute-start(f32[4,256]{1,0:T(4,128)S(1)} %get-tuple-element.174), channel_id=1, source_target_pairs={{0,18},{1,19},{2,20},{3,21},{4,22},{5,23},{6,24},{7,25},{8,26},{9,... | collective-permute-start | bytes 12296 | tf_op jit(solution)/shard_map/ppermute | solution.py:28
  18.4 9.6 %collective-permute-start.11 = (f32[4,256]{1,0:T(4,128)S(1)}, f32[4,256]{1,0:T(4,128)S(1)}, u32[]{:S(2)}, u32[]{:S(2)}) collective-permute-start(f32[4,256]{1,0:T(4,128)S(1)} %get-tuple-element.174), channel_id=1, source_target_pairs={{0,20},{1,21},{2,22},{3,23},{4,24},{5,25},{6,26},{7,27},{8,28},{9,... | collective-permute-start | bytes 12296 | tf_op jit(solution)/shard_map/ppermute | solution.py:28
  28.0 8.7 %collective-permute-start.9 = (f32[4,256]{1,0:T(4,128)S(1)}, f32[4,256]{1,0:T(4,128)S(1)}, u32[]{:S(2)}, u32[]{:S(2)}) collective-permute-start(f32[4,256]{1,0:T(4,128)S(1)} %get-tuple-element.174), channel_id=1, source_target_pairs={{0,22},{1,23},{2,24},{3,25},{4,26},{5,27},{6,28},{7,29},{8,30},{9,... | collective-permute-start | bytes 12296 | tf_op jit(solution)/shard_map/ppermute | solution.py:28
  44.0 3.8 collective-permute-start.5
  47.9 6.0 %collective-permute-start.3 = (f32[4,256]{1,0:T(4,128)S(1)}, f32[4,256]{1,0:T(4,128)S(1)}, u32[]{:S(2)}, u32[]{:S(2)}) collective-permute-start(f32[4,256]{1,0:T(4,128)S(1)} %get-tuple-element.174), channel_id=1, source_target_pairs={{0,28},{1,29},{2,30},{3,31},{4,0},{5,1},{6,2},{7,3},{8,4},{9,5},{1... | collective-permute-start | bytes 12296 | tf_op jit(solution)/shard_map/ppermute | solution.py:28
  53.8 5.1 %collective-permute-start.1 = (f32[4,256]{1,0:T(4,128)S(1)}, f32[4,256]{1,0:T(4,128)S(1)}, u32[]{:S(2)}, u32[]{:S(2)}) collective-permute-start(f32[4,256]{1,0:T(4,128)S(1)} %get-tuple-element.174), channel_id=1, source_target_pairs={{0,30},{1,31},{2,0},{3,1},{4,2},{5,3},{6,4},{7,5},{8,6},{9,7},{10,... | collective-permute-start | bytes 12296 | tf_op jit(solution)/shard_map/ppermute | solution.py:28
  93.8 3.3 collective-permute-start.21
  98.7 6.4 %collective-permute-done.20 = bf16[256,1024]{1,0:T(8,128)(2,1)S(1)} collective-permute-done((bf16[256,1024]{1,0:T(8,128)(2,1)S(1)}, bf16[256,1024]{1,0:T(8,128)(2,1)S(1)}, u32[]{:S(2)}, u32[]{:S(2)}) %collective-permute-start.20) | collective-permute-done | bytes 524320 | tf_op jit(solution)/shard_map/ppermute | solution.py:28
  105.1 3.5 collective-permute-start.28
  108.5 7.8 %collective-permute-done.19 = bf16[256,1024]{1,0:T(8,128)(2,1)S(1)} collective-permute-done((bf16[256,1024]{1,0:T(8,128)(2,1)}, bf16[256,1024]{1,0:T(8,128)(2,1)S(1)}, u32[]{:S(2)}, u32[]{:S(2)}) %collective-permute-start.19) | collective-permute-done | bytes 524320 | tf_op jit(solution)/shard_map/ppermute | solution.py:28
  116.8 3.3 collective-permute-start.27
  120.7 6.9 %collective-permute-done.26 = bf16[256,1024]{1,0:T(8,128)(2,1)} collective-permute-done((bf16[256,1024]{1,0:T(8,128)(2,1)S(1)}, bf16[256,1024]{1,0:T(8,128)(2,1)}, u32[]{:S(2)}, u32[]{:S(2)}) %collective-permute-start.26) | collective-permute-done | bytes 524320 | tf_op jit(solution)/shard_map/ppermute | solution.py:28
  127.7 3.5 collective-permute-start.32
  131.1 7.8 %collective-permute-done.25 = bf16[256,1024]{1,0:T(8,128)(2,1)} collective-permute-done((bf16[256,1024]{1,0:T(8,128)(2,1)S(1)}, bf16[256,1024]{1,0:T(8,128)(2,1)}, u32[]{:S(2)}, u32[]{:S(2)}) %collective-permute-start.25) | collective-permute-done | bytes 524320 | tf_op jit(solution)/shard_map/ppermute | solution.py:28
  141.6 3.8 collective-permute-start.31
  153.0 8.2 %fusion.24 = bf16[320,2048]{1,0:T(8,128)(2,1)} fusion(bf16[1,1024,2048]{2,1,0:T(8,128)(2,1)} %param.13, f32[320,1024]{1,0:T(8,128)} %fusion.14, bf16[320,2048]{1,0:T(8,128)(2,1)} %copy-done.61, bf16[1,2048,1024]{2,1,0:T(8,128)(2,1)} %param.11), kind=kOutput, calls=%fused_computation.24 | convolution fusion | flops 2686976000 | bytes 12320768 | tf_op jit(solution)/shard_map/dot_general | solution.py:12
  182.8 5.1 %collective-permute-done.35 = bf16[224,1024]{1,0:T(8,128)(2,1)S(1)} collective-permute-done((bf16[224,1024]{1,0:T(8,128)(2,1)S(1)}, bf16[224,1024]{1,0:T(8,128)(2,1)S(1)}, u32[]{:S(2)}, u32[]{:S(2)}) %collective-permute-start.35) | collective-permute-done | bytes 458784 | tf_op jit(solution)/shard_map/ppermute | solution.py:28
  189.4 3.4 collective-permute-start.41
  198.2 6.5 %fusion.27 = bf16[256,2048]{1,0:T(8,128)(2,1)S(1)} fusion(bf16[1,1024,2048]{2,1,0:T(8,128)(2,1)} %param.13, f32[256,1024]{1,0:T(8,128)} %fusion.12, bf16[256,2048]{1,0:T(8,128)(2,1)} %copy-done.57, bf16[1,2048,1024]{2,1,0:T(8,128)(2,1)} %param.11), kind=kOutput, calls=%fused_computation.25 | convolution fusion | flops 2149580800 | bytes 11534336 | tf_op jit(solution)/shard_map/dot_general | solution.py:12
  214.2 3.3 collective-permute-start.52
  233.3 7.4 %fusion.30 = bf16[256,2048]{1,0:T(8,128)(2,1)} fusion(bf16[1,1024,2048]{2,1,0:T(8,128)(2,1)} %param.13, f32[256,1024]{1,0:T(8,128)} %fusion.10, bf16[256,2048]{1,0:T(8,128)(2,1)} %copy-done.59, bf16[1,2048,1024]{2,1,0:T(8,128)(2,1)} %param.11), kind=kOutput, calls=%fused_computation.26 | convolution fusion | flops 2149580800 | bytes 11534336 | tf_op jit(solution)/shard_map/dot_general | solution.py:12
  244.7 4.2 %fusion.8 = f32[192,1024]{1,0:T(8,128)} fusion(bf16[1,2048,1024]{2,1,0:T(8,128)(2,1)} %param.12, bf16[96,2048]{1,0:T(8,128)(2,1)} %collective-permute-done.53, bf16[32,2048]{1,0:T(8,128)(2,1)S(1)} %copy-done.41, bf16[32,2048]{1,0:T(8,128)(2,1)S(1)} %copy-done.40, bf16[32,2048]{1,0:T(8,128)(2,1)S(1)} %copy-done.39), kind=kOutput, calls=%fused_computation.8 | convolution fusion | flops 808452096 | bytes 5767168 | tf_op jit(solution)/shard_map/dot_general | solution.py:12
  248.9 6.7 %fusion.33 = bf16[192,2048]{1,0:T(8,128)(2,1)} fusion(bf16[1,1024,2048]{2,1,0:T(8,128)(2,1)} %param.13, f32[192,1024]{1,0:T(8,128)} %fusion.8, bf16[1,2048,1024]{2,1,0:T(8,128)(2,1)} %param.11, bf16[96,2048]{1,0:T(8,128)(2,1)} %collective-permute-done.53, bf16[32,2048]{1,0:T(8,128)(2,1)} %get-tuple-element.130, bf16[32,2048]{1,0:T(8,128)(2,1)} %fusion.329, ...), kind=kOutput, calls=%fused_computation.27 | convolution fusion | flops 1615331328 | bytes 10747904 | tf_op jit(solution)/shard_map/dot_general | solution.py:12
  258.8 3.4 collective-permute-start.55
  264.8 3.8 collective-permute-start.56
  271.7 3.9 collective-permute-done.72
  275.8 3.8 collective-permute-start.73
  285.8 7.7 %collective-permute-done.65 = bf16[160,1024]{1,0:T(8,128)(2,1)S(1)} collective-permute-done((bf16[160,1024]{1,0:T(8,128)(2,1)S(1)}, bf16[160,1024]{1,0:T(8,128)(2,1)S(1)}, u32[]{:S(2)}, u32[]{:S(2)}) %collective-permute-start.65) | collective-permute-done | bytes 327712 | tf_op jit(solution)/shard_map/ppermute | solution.py:28
  294.0 6.6 %collective-permute-done.81 = bf16[160,1024]{1,0:T(8,128)(2,1)S(1)} collective-permute-done((bf16[160,1024]{1,0:T(8,128)(2,1)S(1)}, bf16[160,1024]{1,0:T(8,128)(2,1)S(1)}, u32[]{:S(2)}, u32[]{:S(2)}) %collective-permute-start.81) | collective-permute-done | bytes 327712 | tf_op jit(solution)/shard_map/ppermute | solution.py:28
  305.1 5.3 %collective-permute-done.66 = bf16[224,1024]{1,0:T(8,128)(2,1)S(1)} collective-permute-done((bf16[224,1024]{1,0:T(8,128)(2,1)S(1)}, bf16[224,1024]{1,0:T(8,128)(2,1)S(1)}, u32[]{:S(2)}, u32[]{:S(2)}) %collective-permute-start.66) | collective-permute-done | bytes 458784 | tf_op jit(solution)/shard_map/ppermute | solution.py:28
  310.9 4.7 %collective-permute-done.74 = bf16[224,1024]{1,0:T(8,128)(2,1)S(1)} collective-permute-done((bf16[224,1024]{1,0:T(8,128)(2,1)S(1)}, bf16[224,1024]{1,0:T(8,128)(2,1)S(1)}, u32[]{:S(2)}, u32[]{:S(2)}) %collective-permute-start.74) | collective-permute-done | bytes 458784 | tf_op jit(solution)/shard_map/ppermute | solution.py:28
  315.9 3.8 collective-permute-start.75
  319.7 5.6 %collective-permute-done.58 = bf16[224,1024]{1,0:T(8,128)(2,1)S(1)} collective-permute-done((bf16[224,1024]{1,0:T(8,128)(2,1)S(1)}, bf16[224,1024]{1,0:T(8,128)(2,1)S(1)}, u32[]{:S(2)}, u32[]{:S(2)}) %collective-permute-start.58) | collective-permute-done | bytes 458784 | tf_op jit(solution)/shard_map/ppermute | solution.py:28
  325.7 3.8 collective-permute-start.59
  330.1 6.5 %collective-permute-done.75 = bf16[256,1024]{1,0:T(8,128)(2,1)S(1)} collective-permute-done((bf16[256,1024]{1,0:T(8,128)(2,1)S(1)}, bf16[256,1024]{1,0:T(8,128)(2,1)S(1)}, u32[]{:S(2)}, u32[]{:S(2)}) %collective-permute-start.75) | collective-permute-done | bytes 524320 | tf_op jit(solution)/shard_map/ppermute | solution.py:28
  336.9 3.8 collective-permute-start.76
  340.7 7.1 %collective-permute-done.59 = bf16[256,1024]{1,0:T(8,128)(2,1)S(1)} collective-permute-done((bf16[256,1024]{1,0:T(8,128)(2,1)S(1)}, bf16[256,1024]{1,0:T(8,128)(2,1)S(1)}, u32[]{:S(2)}, u32[]{:S(2)}) %collective-permute-start.59) | collective-permute-done | bytes 524320 | tf_op jit(solution)/shard_map/ppermute | solution.py:28
  348.2 3.8 collective-permute-start.60
  352.9 6.1 %collective-permute-done.76 = bf16[256,1024]{1,0:T(8,128)(2,1)S(1)} collective-permute-done((bf16[256,1024]{1,0:T(8,128)(2,1)S(1)}, bf16[256,1024]{1,0:T(8,128)(2,1)S(1)}, u32[]{:S(2)}, u32[]{:S(2)}) %collective-permute-start.76) | collective-permute-done | bytes 524320 | tf_op jit(solution)/shard_map/ppermute | solution.py:28
  359.4 3.8 collective-permute-start.77
  363.2 7.1 %collective-permute-done.60 = bf16[256,1024]{1,0:T(8,128)(2,1)S(1)} collective-permute-done((bf16[256,1024]{1,0:T(8,128)(2,1)S(1)}, bf16[256,1024]{1,0:T(8,128)(2,1)S(1)}, u32[]{:S(2)}, u32[]{:S(2)}) %collective-permute-start.60) | collective-permute-done | bytes 524320 | tf_op jit(solution)/shard_map/ppermute | solution.py:28
  370.6 3.8 collective-permute-start.61
  375.4 6.1 %collective-permute-done.77 = bf16[256,1024]{1,0:T(8,128)(2,1)S(1)} collective-permute-done((bf16[256,1024]{1,0:T(8,128)(2,1)S(1)}, bf16[256,1024]{1,0:T(8,128)(2,1)S(1)}, u32[]{:S(2)}, u32[]{:S(2)}) %collective-permute-start.77) | collective-permute-done | bytes 524320 | tf_op jit(solution)/shard_map/ppermute | solution.py:28
  381.9 4.3 %collective-permute-start.78 = (bf16[256,1024]{1,0:T(8,128)(2,1)S(1)}, bf16[256,1024]{1,0:T(8,128)(2,1)S(1)}, u32[]{:S(2)}, u32[]{:S(2)}) collective-permute-start(bf16[256,1024]{1,0:T(8,128)(2,1)S(1)} %add_convert_fusion.4), channel_id=1, source_target_pairs={{0,30},{1,31},{2,0},{3,1},{4,2},{5,3},{6,4},{7,5},{8,6},{9,7},{10,... | collective-permute-start | bytes 1572872 | tf_op jit(solution)/shard_map/ppermute | solution.py:28
  386.1 6.6 %collective-permute-done.61 = bf16[256,1024]{1,0:T(8,128)(2,1)S(1)} collective-permute-done((bf16[256,1024]{1,0:T(8,128)(2,1)S(1)}, bf16[256,1024]{1,0:T(8,128)(2,1)S(1)}, u32[]{:S(2)}, u32[]{:S(2)}) %collective-permute-start.61) | collective-permute-done | bytes 524320 | tf_op jit(solution)/shard_map/ppermute | solution.py:28
  393.1 3.8 collective-permute-start.62
  398.5 9.4 %collective-permute-done.62 = bf16[256,1024]{1,0:T(8,128)(2,1)S(1)} collective-permute-done((bf16[256,1024]{1,0:T(8,128)(2,1)S(1)}, bf16[256,1024]{1,0:T(8,128)(2,1)S(1)}, u32[]{:S(2)}, u32[]{:S(2)}) %collective-permute-start.62) | collective-permute-done | bytes 524320 | tf_op jit(solution)/shard_map/ppermute | solution.py:28
  408.1 5.2 %collective-permute-done.86 = bf16[256,1024]{1,0:T(8,128)(2,1)S(1)} collective-permute-done((bf16[256,1024]{1,0:T(8,128)(2,1)S(1)}, bf16[256,1024]{1,0:T(8,128)(2,1)S(1)}, u32[]{:S(2)}, u32[]{:S(2)}) %collective-permute-start.86) | collective-permute-done | bytes 524320 | tf_op jit(solution)/shard_map/ppermute | solution.py:28
  (525 shorter events, 143.3 us)
Async XLA Ops:
  3.1 34.8 %collective-permute-start.13 = (f32[4,256]{1,0:T(4,128)S(1)}, f32[4,256]{1,0:T(4,128)S(1)}, u32[]{:S(2)}, u32[]{:S(2)}) collective-permute-start(f32[4,256]{1,0:T(4,128)S(1)} %get-tuple-element.174), channel_id=1, source_target_pairs={{0,18},{1,19},{2,20},{3,21},{4,22},{5,23},{6,24},{7,25},{8,26},{9,... | collective-permute-start | bytes 12296 | tf_op jit(solution)/shard_map/ppermute | solution.py:28
  18.4 19.6 %collective-permute-start.12 = (f32[4,256]{1,0:T(4,128)S(1)}, f32[4,256]{1,0:T(4,128)S(1)}, u32[]{:S(2)}, u32[]{:S(2)}) collective-permute-start(f32[4,256]{1,0:T(4,128)S(1)} %get-tuple-element.174), channel_id=1, source_target_pairs={{0,14},{1,15},{2,16},{3,17},{4,18},{5,19},{6,20},{7,21},{8,22},{9,... | collective-permute-start | bytes 12296 | tf_op jit(solution)/shard_map/ppermute | solution.py:28
  18.4 22.5 %collective-permute-start.11 = (f32[4,256]{1,0:T(4,128)S(1)}, f32[4,256]{1,0:T(4,128)S(1)}, u32[]{:S(2)}, u32[]{:S(2)}) collective-permute-start(f32[4,256]{1,0:T(4,128)S(1)} %get-tuple-element.174), channel_id=1, source_target_pairs={{0,20},{1,21},{2,22},{3,23},{4,24},{5,25},{6,26},{7,27},{8,28},{9,... | collective-permute-start | bytes 12296 | tf_op jit(solution)/shard_map/ppermute | solution.py:28
  28.0 19.8 %collective-permute-start.9 = (f32[4,256]{1,0:T(4,128)S(1)}, f32[4,256]{1,0:T(4,128)S(1)}, u32[]{:S(2)}, u32[]{:S(2)}) collective-permute-start(f32[4,256]{1,0:T(4,128)S(1)} %get-tuple-element.174), channel_id=1, source_target_pairs={{0,22},{1,23},{2,24},{3,25},{4,26},{5,27},{6,28},{7,29},{8,30},{9,... | collective-permute-start | bytes 12296 | tf_op jit(solution)/shard_map/ppermute | solution.py:28
  62.0 26.9 %collective-permute-start.16 = (bf16[256,1024]{1,0:T(8,128)(2,1)}, bf16[256,1024]{1,0:T(8,128)(2,1)S(1)}, u32[]{:S(2)}, u32[]{:S(2)}) collective-permute-start(bf16[256,1024]{1,0:T(8,128)(2,1)} %get-tuple-element.26), channel_id=1, source_target_pairs={{0,2},{1,3},{2,4},{3,5},{4,6},{5,7},{6,8},{7,9},{8,10},{9,11},{10,... | collective-permute-start | bytes 1572872 | tf_op jit(solution)/shard_map/ppermute | solution.py:28
  63.5 25.6 %collective-permute-start.18 = (bf16[256,1024]{1,0:T(8,128)(2,1)}, bf16[256,1024]{1,0:T(8,128)(2,1)}, u32[]{:S(2)}, u32[]{:S(2)}) collective-permute-start(bf16[256,1024]{1,0:T(8,128)(2,1)} %get-tuple-element.26), channel_id=1, source_target_pairs={{0,30},{1,31},{2,0},{3,1},{4,2},{5,3},{6,4},{7,5},{8,6},{9,7},{10,... | collective-permute-start | bytes 1572872 | tf_op jit(solution)/shard_map/ppermute | solution.py:28
  65.5 26.8 %collective-permute-start.15 = (bf16[256,1024]{1,0:T(8,128)(2,1)}, bf16[256,1024]{1,0:T(8,128)(2,1)}, u32[]{:S(2)}, u32[]{:S(2)}) collective-permute-start(bf16[256,1024]{1,0:T(8,128)(2,1)} %get-tuple-element.27), channel_id=1, source_target_pairs={{0,2},{1,3},{2,4},{3,5},{4,6},{5,7},{6,8},{7,9},{8,10},{9,11},{10,... | collective-permute-start | bytes 1572872 | tf_op jit(solution)/shard_map/ppermute | solution.py:28
  66.2 27.7 %collective-permute-start.17 = (bf16[256,1024]{1,0:T(8,128)(2,1)}, bf16[256,1024]{1,0:T(8,128)(2,1)S(1)}, u32[]{:S(2)}, u32[]{:S(2)}) collective-permute-start(bf16[256,1024]{1,0:T(8,128)(2,1)} %get-tuple-element.27), channel_id=1, source_target_pairs={{0,30},{1,31},{2,0},{3,1},{4,2},{5,3},{6,4},{7,5},{8,6},{9,7},{10,... | collective-permute-start | bytes 1572872 | tf_op jit(solution)/shard_map/ppermute | solution.py:28
  92.3 24.0 %collective-permute-start.19 = (bf16[256,1024]{1,0:T(8,128)(2,1)}, bf16[256,1024]{1,0:T(8,128)(2,1)S(1)}, u32[]{:S(2)}, u32[]{:S(2)}) collective-permute-start(bf16[256,1024]{1,0:T(8,128)(2,1)} %collective-permute-done.15), channel_id=1, source_target_pairs={{0,2},{1,3},{2,4},{3,5},{4,6},{5,7},{6,8},{7,9},{8,10},{9,11},{10,... | collective-permute-start | bytes 1572872 | tf_op jit(solution)/shard_map/ppermute | solution.py:28
  93.8 22.9 %collective-permute-start.21 = (bf16[256,1024]{1,0:T(8,128)(2,1)S(1)}, bf16[256,1024]{1,0:T(8,128)(2,1)S(1)}, u32[]{:S(2)}, u32[]{:S(2)}) collective-permute-start(bf16[256,1024]{1,0:T(8,128)(2,1)S(1)} %collective-permute-done.17), channel_id=1, source_target_pairs={{0,30},{1,31},{2,0},{3,1},{4,2},{5,3},{6,4},{7,5},{8,6},{9,7},{10,... | collective-permute-start | bytes 1572872 | tf_op jit(solution)/shard_map/ppermute | solution.py:28
  105.1 22.6 %collective-permute-start.26 = (bf16[256,1024]{1,0:T(8,128)(2,1)S(1)}, bf16[256,1024]{1,0:T(8,128)(2,1)}, u32[]{:S(2)}, u32[]{:S(2)}) collective-permute-start(bf16[256,1024]{1,0:T(8,128)(2,1)S(1)} %collective-permute-done.20), channel_id=1, source_target_pairs={{0,2},{1,3},{2,4},{3,5},{4,6},{5,7},{6,8},{7,9},{8,10},{9,11},{10,... | collective-permute-start | bytes 1572872 | tf_op jit(solution)/shard_map/ppermute | solution.py:28
  105.1 22.6 %collective-permute-start.28 = (bf16[256,1024]{1,0:T(8,128)(2,1)S(1)}, bf16[256,1024]{1,0:T(8,128)(2,1)}, u32[]{:S(2)}, u32[]{:S(2)}) collective-permute-start(bf16[256,1024]{1,0:T(8,128)(2,1)S(1)} %collective-permute-done.22), channel_id=1, source_target_pairs={{0,30},{1,31},{2,0},{3,1},{4,2},{5,3},{6,4},{7,5},{8,6},{9,7},{10,... | collective-permute-start | bytes 1572872 | tf_op jit(solution)/shard_map/ppermute | solution.py:28
  116.3 22.6 %collective-permute-start.25 = (bf16[256,1024]{1,0:T(8,128)(2,1)S(1)}, bf16[256,1024]{1,0:T(8,128)(2,1)}, u32[]{:S(2)}, u32[]{:S(2)}) collective-permute-start(bf16[256,1024]{1,0:T(8,128)(2,1)S(1)} %collective-permute-done.19), channel_id=1, source_target_pairs={{0,2},{1,3},{2,4},{3,5},{4,6},{5,7},{6,8},{7,9},{8,10},{9,11},{10,... | collective-permute-start | bytes 1572872 | tf_op jit(solution)/shard_map/ppermute | solution.py:28
  116.8 24.8 %collective-permute-start.27 = (bf16[256,1024]{1,0:T(8,128)(2,1)S(1)}, bf16[256,1024]{1,0:T(8,128)(2,1)}, u32[]{:S(2)}, u32[]{:S(2)}) collective-permute-start(bf16[256,1024]{1,0:T(8,128)(2,1)S(1)} %collective-permute-done.21), channel_id=1, source_target_pairs={{0,30},{1,31},{2,0},{3,1},{4,2},{5,3},{6,4},{7,5},{8,6},{9,7},{10,... | collective-permute-start | bytes 1572872 | tf_op jit(solution)/shard_map/ppermute | solution.py:28
  120.6 28.6 %collective-permute-start.23 = (bf16[160,2048]{1,0:T(8,128)(2,1)S(1)}, bf16[160,2048]{1,0:T(8,128)(2,1)S(1)}, u32[]{:S(2)}, u32[]{:S(2)}) collective-permute-start(bf16[160,2048]{1,0:T(8,128)(2,1)S(1)} %get-tuple-element.111), channel_id=1, source_target_pairs={{0,1},{1,0},{2,3},{3,2},{4,5},{5,4},{6,7},{7,6},{8,9},{9,8},{10,11... | collective-permute-start | bytes 1966088 | tf_op jit(solution)/shard_map/ppermute | solution.py:31
  127.7 35.4 %collective-permute-start.30 = (bf16[256,1024]{1,0:T(8,128)(2,1)}, bf16[256,1024]{1,0:T(8,128)(2,1)S(1)}, u32[]{:S(2)}, u32[]{:S(2)}) collective-permute-start(bf16[256,1024]{1,0:T(8,128)(2,1)} %collective-permute-done.26), channel_id=1, source_target_pairs={{0,2},{1,3},{2,4},{3,5},{4,6},{5,7},{6,8},{7,9},{8,10},{9,11},{10,... | collective-permute-start | bytes 1572872 | tf_op jit(solution)/shard_map/ppermute | solution.py:28
  127.7 35.8 %collective-permute-start.32 = (bf16[256,1024]{1,0:T(8,128)(2,1)}, bf16[256,1024]{1,0:T(8,128)(2,1)S(1)}, u32[]{:S(2)}, u32[]{:S(2)}) collective-permute-start(bf16[256,1024]{1,0:T(8,128)(2,1)} %collective-permute-done.28), channel_id=1, source_target_pairs={{0,30},{1,31},{2,0},{3,1},{4,2},{5,3},{6,4},{7,5},{8,6},{9,7},{10,... | collective-permute-start | bytes 1572872 | tf_op jit(solution)/shard_map/ppermute | solution.py:28
  138.9 28.2 %collective-permute-start.29 = (bf16[256,1024]{1,0:T(8,128)(2,1)}, bf16[256,1024]{1,0:T(8,128)(2,1)S(1)}, u32[]{:S(2)}, u32[]{:S(2)}) collective-permute-start(bf16[256,1024]{1,0:T(8,128)(2,1)} %collective-permute-done.25), channel_id=1, source_target_pairs={{0,2},{1,3},{2,4},{3,5},{4,6},{5,7},{6,8},{7,9},{8,10},{9,11},{10,... | collective-permute-start | bytes 1572872 | tf_op jit(solution)/shard_map/ppermute | solution.py:28
  141.6 26.0 %collective-permute-start.31 = (bf16[256,1024]{1,0:T(8,128)(2,1)}, bf16[256,1024]{1,0:T(8,128)(2,1)S(1)}, u32[]{:S(2)}, u32[]{:S(2)}) collective-permute-start(bf16[256,1024]{1,0:T(8,128)(2,1)} %collective-permute-done.27), channel_id=1, source_target_pairs={{0,30},{1,31},{2,0},{3,1},{4,2},{5,3},{6,4},{7,5},{8,6},{9,7},{10,... | collective-permute-start | bytes 1572872 | tf_op jit(solution)/shard_map/ppermute | solution.py:28
  167.4 20.5 %collective-permute-start.35 = (bf16[224,1024]{1,0:T(8,128)(2,1)S(1)}, bf16[224,1024]{1,0:T(8,128)(2,1)S(1)}, u32[]{:S(2)}, u32[]{:S(2)}) collective-permute-start(bf16[224,1024]{1,0:T(8,128)(2,1)S(1)} %convolution_convert_fusion.3), channel_id=1, source_target_pairs={{0,2},{1,3},{2,4},{3,5},{4,6},{5,7},{6,8},{7,9},{8,10},{9,11},{10,... | collective-permute-start | bytes 1376264 | tf_op jit(solution)/shard_map/ppermute | solution.py:28
  167.9 20.8 %collective-permute-start.37 = (bf16[224,1024]{1,0:T(8,128)(2,1)S(1)}, bf16[224,1024]{1,0:T(8,128)(2,1)S(1)}, u32[]{:S(2)}, u32[]{:S(2)}) collective-permute-start(bf16[224,1024]{1,0:T(8,128)(2,1)S(1)} %convolution_convert_fusion.1), channel_id=1, source_target_pairs={{0,30},{1,31},{2,0},{3,1},{4,2},{5,3},{6,4},{7,5},{8,6},{9,7},{10,... | collective-permute-start | bytes 1376264 | tf_op jit(solution)/shard_map/ppermute | solution.py:28
  172.2 22.8 %collective-permute-start.33 = (bf16[128,2048]{1,0:T(8,128)(2,1)S(1)}, bf16[128,2048]{1,0:T(8,128)(2,1)S(1)}, u32[]{:S(2)}, u32[]{:S(2)}) collective-permute-start(bf16[128,2048]{1,0:T(8,128)(2,1)S(1)} %fusion.126), channel_id=1, source_target_pairs={{0,1},{1,0},{2,3},{3,2},{4,5},{5,4},{6,7},{7,6},{8,9},{9,8},{10,11... | collective-permute-start | bytes 1572872 | tf_op jit(solution)/shard_map/ppermute | solution.py:31
  178.8 26.2 %collective-permute-start.40 = (bf16[160,1024]{1,0:T(8,128)(2,1)}, bf16[160,1024]{1,0:T(8,128)(2,1)S(1)}, u32[]{:S(2)}, u32[]{:S(2)}) collective-permute-start(bf16[160,1024]{1,0:T(8,128)(2,1)} %slice.1138), channel_id=1, source_target_pairs={{0,2},{1,3},{2,4},{3,5},{4,6},{5,7},{6,8},{7,9},{8,10},{9,11},{10,... | collective-permute-start | bytes 983048 | tf_op jit(solution)/shard_map/ppermute | solution.py:28
  179.6 25.6 %collective-permute-start.42 = (bf16[160,1024]{1,0:T(8,128)(2,1)}, bf16[160,1024]{1,0:T(8,128)(2,1)S(1)}, u32[]{:S(2)}, u32[]{:S(2)}) collective-permute-start(bf16[160,1024]{1,0:T(8,128)(2,1)} %slice.1148), channel_id=1, source_target_pairs={{0,30},{1,31},{2,0},{3,1},{4,2},{5,3},{6,4},{7,5},{8,6},{9,7},{10,... | collective-permute-start | bytes 983048 | tf_op jit(solution)/shard_map/ppermute | solution.py:28
  188.6 19.8 %collective-permute-start.39 = (bf16[160,1024]{1,0:T(8,128)(2,1)}, bf16[160,1024]{1,0:T(8,128)(2,1)S(1)}, u32[]{:S(2)}, u32[]{:S(2)}) collective-permute-start(bf16[160,1024]{1,0:T(8,128)(2,1)} %slice.1136), channel_id=1, source_target_pairs={{0,2},{1,3},{2,4},{3,5},{4,6},{5,7},{6,8},{7,9},{8,10},{9,11},{10,... | collective-permute-start | bytes 983048 | tf_op jit(solution)/shard_map/ppermute | solution.py:28
  189.4 19.2 %collective-permute-start.41 = (bf16[160,1024]{1,0:T(8,128)(2,1)}, bf16[160,1024]{1,0:T(8,128)(2,1)S(1)}, u32[]{:S(2)}, u32[]{:S(2)}) collective-permute-start(bf16[160,1024]{1,0:T(8,128)(2,1)} %slice.1146), channel_id=1, source_target_pairs={{0,30},{1,31},{2,0},{3,1},{4,2},{5,3},{6,4},{7,5},{8,6},{9,7},{10,... | collective-permute-start | bytes 983048 | tf_op jit(solution)/shard_map/ppermute | solution.py:28
  204.8 21.3 %collective-permute-start.34 = (bf16[128,2048]{1,0:T(8,128)(2,1)S(1)}, bf16[128,2048]{1,0:T(8,128)(2,1)S(1)}, u32[]{:S(2)}, u32[]{:S(2)}) collective-permute-start(bf16[128,2048]{1,0:T(8,128)(2,1)S(1)} %slice.1086), channel_id=1, source_target_pairs={{0,1},{1,0},{2,3},{3,2},{4,5},{5,4},{6,7},{7,6},{8,9},{9,8},{10,11... | collective-permute-start | bytes 1572872 | tf_op jit(solution)/shard_map/ppermute | solution.py:31
  225.4 19.2 %collective-permute-start.53 = (bf16[96,2048]{1,0:T(8,128)(2,1)}, bf16[96,2048]{1,0:T(8,128)(2,1)}, u32[]{:S(2)}, u32[]{:S(2)}) collective-permute-start(bf16[96,2048]{1,0:T(8,128)(2,1)} %fusion.143), channel_id=1, source_target_pairs={{0,1},{1,0},{2,3},{3,2},{4,5},{5,4},{6,7},{7,6},{8,9},{9,8},{10,11... | collective-permute-start | bytes 1179656 | tf_op jit(solution)/shard_map/ppermute | solution.py:31
  264.8 17.4 %collective-permute-start.56 = (bf16[96,1024]{1,0:T(8,128)(2,1)S(1)}, bf16[96,1024]{1,0:T(8,128)(2,1)S(1)}, u32[]{:S(2)}, u32[]{:S(2)}) collective-permute-start(bf16[96,1024]{1,0:T(8,128)(2,1)S(1)} %add_convert_fusion.25), channel_id=1, source_target_pairs={{0,30},{1,31},{2,0},{3,1},{4,2},{5,3},{6,4},{7,5},{8,6},{9,7},{10,... | collective-permute-start | bytes 589832 | tf_op jit(solution)/shard_map/ppermute | solution.py:28
  275.8 25.2 %collective-permute-start.73 = (bf16[160,1024]{1,0:T(8,128)(2,1)S(1)}, bf16[160,1024]{1,0:T(8,128)(2,1)S(1)}, u32[]{:S(2)}, u32[]{:S(2)}) collective-permute-start(bf16[160,1024]{1,0:T(8,128)(2,1)S(1)} %add_convert_fusion.19), channel_id=1, source_target_pairs={{0,30},{1,31},{2,0},{3,1},{4,2},{5,3},{6,4},{7,5},{8,6},{9,7},{10,... | collective-permute-start | bytes 983048 | tf_op jit(solution)/shard_map/ppermute | solution.py:28
  282.1 18.5 %collective-permute-start.81 = (bf16[160,1024]{1,0:T(8,128)(2,1)S(1)}, bf16[160,1024]{1,0:T(8,128)(2,1)S(1)}, u32[]{:S(2)}, u32[]{:S(2)}) collective-permute-start(bf16[160,1024]{1,0:T(8,128)(2,1)S(1)} %add_convert_fusion.18), channel_id=1, source_target_pairs={{0,2},{1,3},{2,4},{3,5},{4,6},{5,7},{6,8},{7,9},{8,10},{9,11},{10,... | collective-permute-start | bytes 983048 | tf_op jit(solution)/shard_map/ppermute | solution.py:28
  282.5 22.1 %collective-permute-start.57 = (bf16[160,1024]{1,0:T(8,128)(2,1)S(1)}, bf16[160,1024]{1,0:T(8,128)(2,1)S(1)}, u32[]{:S(2)}, u32[]{:S(2)}) collective-permute-start(bf16[160,1024]{1,0:T(8,128)(2,1)S(1)} %add_convert_fusion.21), channel_id=1, source_target_pairs={{0,30},{1,31},{2,0},{3,1},{4,2},{5,3},{6,4},{7,5},{8,6},{9,7},{10,... | collective-permute-start | bytes 983048 | tf_op jit(solution)/shard_map/ppermute | solution.py:28
  293.8 16.5 %collective-permute-start.66 = (bf16[224,1024]{1,0:T(8,128)(2,1)S(1)}, bf16[224,1024]{1,0:T(8,128)(2,1)S(1)}, u32[]{:S(2)}, u32[]{:S(2)}) collective-permute-start(bf16[224,1024]{1,0:T(8,128)(2,1)S(1)} %add_convert_fusion.16), channel_id=1, source_target_pairs={{0,2},{1,3},{2,4},{3,5},{4,6},{5,7},{6,8},{7,9},{8,10},{9,11},{10,... | collective-permute-start | bytes 1376264 | tf_op jit(solution)/shard_map/ppermute | solution.py:28
  300.8 28.7 %collective-permute-start.82 = (bf16[224,1024]{1,0:T(8,128)(2,1)S(1)}, bf16[224,1024]{1,0:T(8,128)(2,1)S(1)}, u32[]{:S(2)}, u32[]{:S(2)}) collective-permute-start(bf16[224,1024]{1,0:T(8,128)(2,1)S(1)} %add_convert_fusion.14), channel_id=1, source_target_pairs={{0,2},{1,3},{2,4},{3,5},{4,6},{5,7},{6,8},{7,9},{8,10},{9,11},{10,... | collective-permute-start | bytes 1376264 | tf_op jit(solution)/shard_map/ppermute | solution.py:28
  304.9 20.4 %collective-permute-start.58 = (bf16[224,1024]{1,0:T(8,128)(2,1)S(1)}, bf16[224,1024]{1,0:T(8,128)(2,1)S(1)}, u32[]{:S(2)}, u32[]{:S(2)}) collective-permute-start(bf16[224,1024]{1,0:T(8,128)(2,1)S(1)} %add_convert_fusion.17), channel_id=1, source_target_pairs={{0,30},{1,31},{2,0},{3,1},{4,2},{5,3},{6,4},{7,5},{8,6},{9,7},{10,... | collective-permute-start | bytes 1376264 | tf_op jit(solution)/shard_map/ppermute | solution.py:28
  310.7 41.2 %collective-permute-start.67 = (bf16[256,1024]{1,0:T(8,128)(2,1)S(1)}, bf16[256,1024]{1,0:T(8,128)(2,1)S(1)}, u32[]{:S(2)}, u32[]{:S(2)}) collective-permute-start(bf16[256,1024]{1,0:T(8,128)(2,1)S(1)} %fusion.37), channel_id=1, source_target_pairs={{0,2},{1,3},{2,4},{3,5},{4,6},{5,7},{6,8},{7,9},{8,10},{9,11},{10,... | collective-permute-start | bytes 1572872 | tf_op jit(solution)/shard_map/ppermute | solution.py:28
  315.9 20.7 %collective-permute-start.75 = (bf16[256,1024]{1,0:T(8,128)(2,1)S(1)}, bf16[256,1024]{1,0:T(8,128)(2,1)S(1)}, u32[]{:S(2)}, u32[]{:S(2)}) collective-permute-start(bf16[256,1024]{1,0:T(8,128)(2,1)S(1)} %fusion.38), channel_id=1, source_target_pairs={{0,30},{1,31},{2,0},{3,1},{4,2},{5,3},{6,4},{7,5},{8,6},{9,7},{10,... | collective-permute-start | bytes 1572872 | tf_op jit(solution)/shard_map/ppermute | solution.py:28
  325.7 22.1 %collective-permute-start.59 = (bf16[256,1024]{1,0:T(8,128)(2,1)S(1)}, bf16[256,1024]{1,0:T(8,128)(2,1)S(1)}, u32[]{:S(2)}, u32[]{:S(2)}) collective-permute-start(bf16[256,1024]{1,0:T(8,128)(2,1)S(1)} %fusion.36), channel_id=1, source_target_pairs={{0,30},{1,31},{2,0},{3,1},{4,2},{5,3},{6,4},{7,5},{8,6},{9,7},{10,... | collective-permute-start | bytes 1572872 | tf_op jit(solution)/shard_map/ppermute | solution.py:28
  329.9 22.5 %collective-permute-start.83 = (bf16[256,1024]{1,0:T(8,128)(2,1)S(1)}, bf16[256,1024]{1,0:T(8,128)(2,1)S(1)}, u32[]{:S(2)}, u32[]{:S(2)}) collective-permute-start(bf16[256,1024]{1,0:T(8,128)(2,1)S(1)} %fusion.39), channel_id=1, source_target_pairs={{0,2},{1,3},{2,4},{3,5},{4,6},{5,7},{6,8},{7,9},{8,10},{9,11},{10,... | collective-permute-start | bytes 1572872 | tf_op jit(solution)/shard_map/ppermute | solution.py:28
  336.9 22.1 %collective-permute-start.76 = (bf16[256,1024]{1,0:T(8,128)(2,1)S(1)}, bf16[256,1024]{1,0:T(8,128)(2,1)S(1)}, u32[]{:S(2)}, u32[]{:S(2)}) collective-permute-start(bf16[256,1024]{1,0:T(8,128)(2,1)S(1)} %add_convert_fusion.6), channel_id=1, source_target_pairs={{0,30},{1,31},{2,0},{3,1},{4,2},{5,3},{6,4},{7,5},{8,6},{9,7},{10,... | collective-permute-start | bytes 1572872 | tf_op jit(solution)/shard_map/ppermute | solution.py:28
  348.2 22.1 %collective-permute-start.60 = (bf16[256,1024]{1,0:T(8,128)(2,1)S(1)}, bf16[256,1024]{1,0:T(8,128)(2,1)S(1)}, u32[]{:S(2)}, u32[]{:S(2)}) collective-permute-start(bf16[256,1024]{1,0:T(8,128)(2,1)S(1)} %add_convert_fusion.13), channel_id=1, source_target_pairs={{0,30},{1,31},{2,0},{3,1},{4,2},{5,3},{6,4},{7,5},{8,6},{9,7},{10,... | collective-permute-start | bytes 1572872 | tf_op jit(solution)/shard_map/ppermute | solution.py:28
  352.3 22.1 %collective-permute-start.68 = (bf16[256,1024]{1,0:T(8,128)(2,1)S(1)}, bf16[256,1024]{1,0:T(8,128)(2,1)S(1)}, u32[]{:S(2)}, u32[]{:S(2)}) collective-permute-start(bf16[256,1024]{1,0:T(8,128)(2,1)S(1)} %add_convert_fusion.10), channel_id=1, source_target_pairs={{0,2},{1,3},{2,4},{3,5},{4,6},{5,7},{6,8},{7,9},{8,10},{9,11},{10,... | collective-permute-start | bytes 1572872 | tf_op jit(solution)/shard_map/ppermute | solution.py:28
  352.8 22.1 %collective-permute-start.84 = (bf16[256,1024]{1,0:T(8,128)(2,1)S(1)}, bf16[256,1024]{1,0:T(8,128)(2,1)S(1)}, u32[]{:S(2)}, u32[]{:S(2)}) collective-permute-start(bf16[256,1024]{1,0:T(8,128)(2,1)S(1)} %add_convert_fusion.3), channel_id=1, source_target_pairs={{0,2},{1,3},{2,4},{3,5},{4,6},{5,7},{6,8},{7,9},{8,10},{9,11},{10,... | collective-permute-start | bytes 1572872 | tf_op jit(solution)/shard_map/ppermute | solution.py:28
  359.4 22.1 %collective-permute-start.77 = (bf16[256,1024]{1,0:T(8,128)(2,1)S(1)}, bf16[256,1024]{1,0:T(8,128)(2,1)S(1)}, u32[]{:S(2)}, u32[]{:S(2)}) collective-permute-start(bf16[256,1024]{1,0:T(8,128)(2,1)S(1)} %add_convert_fusion.5), channel_id=1, source_target_pairs={{0,30},{1,31},{2,0},{3,1},{4,2},{5,3},{6,4},{7,5},{8,6},{9,7},{10,... | collective-permute-start | bytes 1572872 | tf_op jit(solution)/shard_map/ppermute | solution.py:28
  370.6 22.1 %collective-permute-start.61 = (bf16[256,1024]{1,0:T(8,128)(2,1)S(1)}, bf16[256,1024]{1,0:T(8,128)(2,1)S(1)}, u32[]{:S(2)}, u32[]{:S(2)}) collective-permute-start(bf16[256,1024]{1,0:T(8,128)(2,1)S(1)} %add_convert_fusion.12), channel_id=1, source_target_pairs={{0,30},{1,31},{2,0},{3,1},{4,2},{5,3},{6,4},{7,5},{8,6},{9,7},{10,... | collective-permute-start | bytes 1572872 | tf_op jit(solution)/shard_map/ppermute | solution.py:28
  374.8 22.1 %collective-permute-start.69 = (bf16[256,1024]{1,0:T(8,128)(2,1)S(1)}, bf16[256,1024]{1,0:T(8,128)(2,1)S(1)}, u32[]{:S(2)}, u32[]{:S(2)}) collective-permute-start(bf16[256,1024]{1,0:T(8,128)(2,1)S(1)} %add_convert_fusion.9), channel_id=1, source_target_pairs={{0,2},{1,3},{2,4},{3,5},{4,6},{5,7},{6,8},{7,9},{8,10},{9,11},{10,... | collective-permute-start | bytes 1572872 | tf_op jit(solution)/shard_map/ppermute | solution.py:28
  375.3 22.1 %collective-permute-start.85 = (bf16[256,1024]{1,0:T(8,128)(2,1)S(1)}, bf16[256,1024]{1,0:T(8,128)(2,1)S(1)}, u32[]{:S(2)}, u32[]{:S(2)}) collective-permute-start(bf16[256,1024]{1,0:T(8,128)(2,1)S(1)} %add_convert_fusion.2), channel_id=1, source_target_pairs={{0,2},{1,3},{2,4},{3,5},{4,6},{5,7},{6,8},{7,9},{8,10},{9,11},{10,... | collective-permute-start | bytes 1572872 | tf_op jit(solution)/shard_map/ppermute | solution.py:28
  381.9 26.3 %collective-permute-start.78 = (bf16[256,1024]{1,0:T(8,128)(2,1)S(1)}, bf16[256,1024]{1,0:T(8,128)(2,1)S(1)}, u32[]{:S(2)}, u32[]{:S(2)}) collective-permute-start(bf16[256,1024]{1,0:T(8,128)(2,1)S(1)} %add_convert_fusion.4), channel_id=1, source_target_pairs={{0,30},{1,31},{2,0},{3,1},{4,2},{5,3},{6,4},{7,5},{8,6},{9,7},{10,... | collective-permute-start | bytes 1572872 | tf_op jit(solution)/shard_map/ppermute | solution.py:28
  (127 other events, 1458.1 us)

commit v2 on v0

v2 whole, which is shorter than its diff:
```python
import functools

import jax
import jax.numpy as jnp
from jax import lax
from jax.experimental import pallas as pl
from jax.experimental.pallas import tpu as pltpu
from jax.sharding import PartitionSpec as P


BF = jnp.bfloat16
F32 = jnp.float32
TILE = 256
LIMIT = 36 * 2**20
META = 8
VMEM = pl.BlockSpec(memory_space=pltpu.VMEM)
SMEM = pl.BlockSpec(memory_space=pltpu.SMEM)


def dot(a, b, dims=((1,), (0,))):
    return lax.dot_general(a, b, (dims, ((), ())), preferred_element_type=F32)


def earlier(n):
    row = lax.broadcasted_iota(jnp.int32, (n, n), 0)
    col = lax.broadcasted_iota(jnp.int32, (n, n), 1)
    return (row < col).astype(BF)


def select_kernel(cap, plan, ids, gain, *refs):
    count = len(plan)
    packets = refs[:count]
    own_ref = refs[count]
    other_ref = refs[count + 1] if any(both for _, both in plan) else None
    backs = refs[-count:]
    me = ids[0]
    slots = lax.broadcasted_iota(jnp.int32, (cap, 1), 0).astype(F32)
    triangles, chosen, scales = {}, [], []
    for packet, back, (size, both) in zip(packets, backs, plan):
        meta = packet[size : size + META, : max(size, 128)].astype(F32)[:, :size]
        hits = []
        for who in (me, me ^ 1) if both else (me,):
            name = (who + 1).astype(F32)
            hits.append((meta[0:1] == name, meta[1:2] == name))
        marks = [(a | c) for a, c in hits]
        if size not in triangles:
            triangles[size] = earlier(size)
        stacked = jnp.concatenate(
            [m.astype(F32) for m in marks] + [jnp.zeros((META - len(marks), size), F32)], 0
        )
        before = dot(stacked.astype(BF), triangles[size])
        picks, highs, lows = [], [], []
        for k, (a, c) in enumerate(hits):
            slot = jnp.where(marks[k], before[k : k + 1], -1.0)
            pick = slots == slot
            high = jnp.where(a, meta[2:3], 0.0) + jnp.where(c, meta[4:5], 0.0)
            low = jnp.where(a, meta[3:4], 0.0) + jnp.where(c, meta[5:6], 0.0)
            picks.append(pick.astype(F32))
            highs.append(jnp.where(pick, high, 0.0))
            lows.append(jnp.where(pick, low, 0.0))
        pick = jnp.concatenate(picks, 0)
        back[...] = jnp.concatenate(highs + lows, 0).astype(BF)
        scales.append(jnp.sum(pick * (meta[6:7] + meta[7:8]), 1, keepdims=True))
        chosen.append(pick.astype(BF))

    def columns(j, _):
        cols = pl.ds(pl.multiple_of(j * TILE, TILE), TILE)
        twos = 0
        for i, (size, both) in enumerate(plan):
            value = dot(chosen[i], packets[i][0:size, cols])
            value = (value * scales[i] * gain[0:1, cols]).astype(BF)
            own_ref[i * cap : (i + 1) * cap, cols] = value[:cap]
            if both:
                other_ref[twos * cap : (twos + 1) * cap, cols] = value[cap:]
                twos += 1
        return 0

    lax.fori_loop(0, gain.shape[1] // TILE, columns, 0)


def select(cap, plan, me, gain, packets):
    width = gain.shape[1]
    twos = sum(both for _, both in plan)
    outs = [jax.ShapeDtypeStruct((len(plan) * cap, width), BF)]
    if twos:
        outs.append(jax.ShapeDtypeStruct((twos * cap, width), BF))
    outs += [jax.ShapeDtypeStruct(((4 if both else 2) * cap, n), BF) for n, both in plan]
    out = pl.pallas_call(
        functools.partial(select_kernel, cap, plan),
        out_shape=outs,
        in_specs=[SMEM] + [VMEM] * (1 + len(packets)),
        out_specs=[VMEM] * len(outs),
        cost_estimate=pl.CostEstimate(
            flops=sum(4 * cap * n * (width + n) for n, _ in plan),
            bytes_accessed=sum(p.size * 2 for p in packets),
            transcendentals=0,
        ),
        compiler_params=pltpu.CompilerParams(vmem_limit_bytes=LIMIT),
        name="select",
    )(me, gain, *packets)
    return out[0], (out[1] if twos else None), out[len(outs) - len(plan) :]


def compact_kernel(rows, size, chips, info, packet, out, place_ref):
    far = chips // 2
    source, near, way, core = info[0], info[1], info[2], info[3]
    meta_bits = packet[rows : rows + META, 0:rows]
    meta = meta_bits.astype(F32)
    best = jnp.zeros((1, rows), jnp.int32)
    for k in (0, 1):
        expert = meta[k : k + 1].astype(jnp.int32) - 1
        dist = (way * ((expert >> 1) - source) + 2 * chips) & (chips - 1)
        good = (dist < far) | ((dist == far) & ((expert & 1) == core))
        best = jnp.maximum(best, jnp.where(good, dist, 0))
    level = lax.broadcasted_iota(jnp.int32, (META, 1), 0)
    at = (best == (far - level)) & (best > near)
    ind = at.astype(F32)
    before = dot(ind.astype(BF), earlier(rows))
    count = jnp.sum(ind, 1, keepdims=True)
    rank = jnp.zeros((1, rows), F32)
    base = jnp.zeros((1, 1), F32)
    for l in range(META):
        rank = rank + ind[l : l + 1] * (before[l : l + 1] + base + 1.0)
        base = base + count[l : l + 1]
    slot = lax.broadcasted_iota(jnp.int32, (size, 1), 0).astype(F32) + 1.0
    place = (slot == rank).astype(F32).astype(BF)
    place_ref[...] = place

    def columns(j, _):
        cols = pl.ds(pl.multiple_of(j * TILE, TILE), TILE)
        out[0:size, cols] = dot(place, packet[0:rows, cols]).astype(BF)
        return 0

    lax.fori_loop(0, packet.shape[1] // TILE, columns, 0)
    moved = dot(meta_bits, place, ((1,), (1,)))
    filler = packet.shape[1] - size
    out[size : size + META, :] = jnp.concatenate(
        [moved, jnp.zeros((META, filler), F32)], 1
    ).astype(BF)


def compact(rows, size, chips, info, packet):
    return pl.pallas_call(
        functools.partial(compact_kernel, rows, size, chips),
        out_shape=[
            jax.ShapeDtypeStruct((size + META, packet.shape[1]), BF),
            jax.ShapeDtypeStruct((size, rows), BF),
        ],
        in_specs=[SMEM, VMEM],
        out_specs=[VMEM, VMEM],
        cost_estimate=pl.CostEstimate(
            flops=2 * rows * size * packet.shape[1],
            bytes_accessed=4 * packet.size,
            transcendentals=0,
        ),
        compiler_params=pltpu.CompilerParams(vmem_limit_bytes=LIMIT),
        name="compact",
    )(info, packet)


def expert_kernel(counts, outs, *refs):
    inputs = refs[: len(counts)]
    w_gate, w_up, w_down = refs[len(counts) : len(counts) + 3]
    x, total = refs[-2:]
    at = 0
    for ref, count in zip(inputs, counts):
        x[at : at + count, :] = ref[...]
        at += count

    def piece(j):
        cols = pl.ds(pl.multiple_of(j * TILE, TILE), TILE)
        gate = dot(x[...], w_gate[0, :, cols])
        upper = dot(x[...], w_up[0, :, cols])
        hidden = (gate / (1.0 + jnp.exp(-gate)) * upper).astype(BF)
        return dot(hidden, w_down[0, cols, :])

    total[...] = piece(0)

    def more(j, _):
        total[...] += piece(j)
        return 0

    lax.fori_loop(1, w_gate.shape[2] // TILE, more, 0)
    at = 0
    for ref, count in zip(refs[len(counts) + 3 : -2], outs):
        ref[...] = total[at : at + count, :].astype(BF)
        at += count


def expert(owns, others, w_gate, w_up, w_down):
    counts = [o.shape[0] for o in owns + others]
    outs = [sum(o.shape[0] for o in side) for side in (owns, others) if side]
    n, width = sum(counts), owns[0].shape[1]
    hidden = w_gate.shape[2]
    return pl.pallas_call(
        functools.partial(expert_kernel, counts, outs),
        in_specs=[VMEM] * (len(counts) + 3),
        out_specs=[VMEM] * len(outs),
        out_shape=[jax.ShapeDtypeStruct((m, width), BF) for m in outs],
        scratch_shapes=[pltpu.VMEM((n, width), BF), pltpu.VMEM((n, width), F32)],
        cost_estimate=pl.CostEstimate(
            flops=n * 6 * width * hidden,
            bytes_accessed=6 * width * hidden,
            transcendentals=n * hidden,
        ),
        compiler_params=pltpu.CompilerParams(vmem_limit_bytes=LIMIT),
        name="expert",
    )(*owns, *others, w_gate, w_up, w_down)


def per_device(tokens, norm_gain, expert_ids, gate_weights, w_gate, w_up, w_down):
    ep = lax.axis_size("ep")
    chips = ep // 2
    far = chips // 2
    rows, width = tokens.shape
    cap = 2 * rows * expert_ids.shape[1] // ep
    size = {t: min(rows, cap * (2 * (far - t) + 1)) for t in range(1, far + 1)}
    near = max(t for t in size if size[t] == rows)
    me = lax.axis_index("ep").astype(jnp.int32)
    chip, core = me // 2, me % 2
    me_ref = me.reshape(1)
    gain = norm_gain.reshape(1, width)

    def shift(x, hops):
        return lax.ppermute(
            x,
            "ep",
            [(i, (i + 2 * hops * (1 if i % 2 == 0 else -1)) % ep) for i in range(ep)],
        )

    def swap(x):
        return lax.ppermute(x, "ep", [(i, i ^ 1) for i in range(ep)])

    values = tokens.astype(F32)
    scale = lax.rsqrt(jnp.mean(values * values, -1) + 1e-06)[None, :]
    facts = jnp.concatenate([gate_weights.T, scale], 0)
    high = lax.reduce_precision(facts, 8, 7)
    low = facts - high
    names = (expert_ids.T + 1).astype(F32)
    meta = jnp.concatenate(
        [names, high[0:1], low[0:1], high[1:2], low[1:2], high[2:3], low[2:3]], 0
    ).astype(BF)
    local = jnp.concatenate([tokens, jnp.pad(meta, ((0, 0), (0, width - rows)))], 0)
    packet = [local, swap(local)]

    way = 1 - 2 * core
    info = jnp.stack([(chip - way * near) % chips, jnp.int32(near), way, core])
    places = {}
    arrived = {(0, 0): local}
    for t in range(1, far + 1):
        for q in (0, 1):
            x = packet[q]
            if t == near + 1:
                x, places[q] = compact(rows, size[t], chips, info, x)
            elif t > near:
                x = jnp.concatenate([x[: size[t]], x[size[t - 1] :]], 0)
            packet[q] = shift(x, 1)
            arrived[t, q] = packet[q]

    groups = [[0, 1], [2, 3], [4], [5, 6], [far - 1], [far]]
    calls = {"ffn0": [0], "ffn1": [1, 2], "ffn2": [3, 4], "ffn3": [5]}
    backs, taken, results = {}, {}, {}
    for g, group in enumerate(groups):
        keys = [(t, q) for t in group for q in ((0, 1) if t else (0,))]
        plan = tuple((arrived[key].shape[0] - META, key[0] < far) for key in keys)
        own, other, mats = select(cap, plan, me_ref, gain, [arrived[key] for key in keys])
        for key, mat in zip(keys, mats):
            backs[key] = mat
        if other is not None:
            other = swap(other)
        taken[g] = (keys, own, other)
    for call in calls.values():
        done = expert(
            [taken[g][1] for g in call],
            [taken[g][2] for g in call if taken[g][2] is not None],
            w_gate,
            w_up,
            w_down,
        )
        if len(done) > 1:
            done = [done[0], swap(done[1])]
        for i, key in enumerate(key for g in call for key in taken[g][0]):
            pieces = [r[i * cap : (i + 1) * cap] for r in done]
            results[key] = jnp.concatenate(pieces + pieces, 0)

    coming = {}
    for t in range(far, 0, -1):
        for q in (1, 0):
            add = dot(backs[t, q], results[t, q], ((0,), (0,)))
            if t < far:
                got = coming[q]
                if t == near:
                    add = add + dot(places[q], got, ((0,), (0,)))
                else:
                    got = got.astype(F32)
                    add = add + jnp.pad(got, ((0, size[t] - got.shape[0]), (0, 0)))
            coming[q] = shift(add.astype(BF), -1)
    other_way = swap(coming[1])
    total = dot(backs[0, 0], results[0, 0], ((0,), (0,)))
    total = total + coming[0].astype(F32) + other_way.astype(F32)
    return total.astype(BF)


def solution(mesh):
    return jax.shard_map(
        per_device,
        mesh=mesh,
        in_specs=(
            P(("grp", "ep"), None),
            P(),
            P(("grp", "ep"), None),
            P(("grp", "ep"), None),
            P("ep", None, None),
            P("ep", None, None),
            P("ep", None, None),
        ),
        out_specs=P(("grp", "ep"), None),
        check_vma=False,
    )
```

time: 459 us -> 325 us (0.71)
  blocking collectives: 208 us -> 0 us
  starting transfers between devices: 6 us -> 53.6 us
  Pallas kernels: 0 us -> 35.7 us
  waiting for transfers between devices: 190 us -> 214 us
  local copies, waits for them, and re-layouts: 23.6 us -> 6.65 us
  other arithmetic: 14.9 us -> 4.51 us
  matrix products: 16 us -> 8.62 us
    ppermute x0 -> x42, waiting for transfers between devices: none -> 214 us  [the longest x32 212 us: shift(): lax.ppermute(x, 'ep', [(i, (i + 2 * hops * (1 if i % 2 == 0 else -1)) % e...]
    all_to_all x1 -> x0, blocking collectives: 208 us -> none  [per_device(): lax.all_to_all(outgoing, 'ep', split_axis=0, concat_axis=0, tiled=True)]
    all_to_all x1 -> x0, waiting for transfers between devices: 190 us -> none  [per_device(): lax.all_to_all(finished, 'ep', split_axis=0, concat_axis=0, tiled=True)]
    ppermute x0 -> x42, starting transfers between devices: none -> 53.6 us  [the longest x32 51.9 us: shift(): lax.ppermute(x, 'ep', [(i, (i + 2 * hops * (1 if i % 2 == 0 else -1)) % e...]
    pallas_call x0 -> x12, Pallas kernels: none -> 35.7 us  [the longest x4 19.1 us: expert(): pl.pallas_call(functools.partial(expert_kernel, counts, outs), in_specs=[...]
    reduce_sum x3 -> x1, other arithmetic: 11.5 us -> 1.51 us  [per_device(): scale = lax.rsqrt(jnp.mean(values * values, -1) + 1e-06)[None, :]]
    dot_general x3 -> x19, matrix products: 16 us -> 8.62 us  [dot(): return lax.dot_general(a, b, (dims, ((), ())), preferred_element_type=F32)]
    scatter x1 -> x0, local copies, waits for them, and re-layouts: 7.21 us -> none  [per_device(): jnp.zeros((experts * capacity, feature_width), jnp.bfloat16).at[dest]]
  transfers between devices with their start and end apart: 1 -> 42, of which waited for: 1 -> 31; matrix products, arithmetic and copies ran while one was open for 0% -> 2% of each run, Pallas kernels for 0% -> 9%
where the time goes in v2:
time: 325 us; the launch traced here: 324 us
  waiting for transfers between devices  214 us (66%)
  starting transfers between devices  53.6 us (16%)
  Pallas kernels  35.7 us (11%)
  matrix products  8.62 us (3%)
  local copies, waits for them, and re-layouts  6.65 us (2%)
  other arithmetic  4.51 us (1%)
    ppermute x32, waiting for transfers between devices, shift(): lax.ppermute(x, 'ep', [(i, (i + 2 * hops * (1 if i % 2 == 0 else -1)) % e...  212 us
    ppermute x32, starting transfers between devices, shift(): lax.ppermute(x, 'ep', [(i, (i + 2 * hops * (1 if i % 2 == 0 else -1)) % e...  51.9 us
    pallas_call x4, Pallas kernels, expert(): pl.pallas_call(functools.partial(expert_kernel, counts, outs), in_specs=[...  19.1 us
    pallas_call x6, Pallas kernels, select(): pl.pallas_call(functools.partial(select_kernel, cap, plan), out_shape=out...  11.7 us
    dot_general x19, matrix products, dot(): return lax.dot_general(a, b, (dims, ((), ())), preferred_element_type=F32)  8.62 us
  transfers between devices with their start and end apart: 42, of which 31 were waited for; matrix products, arithmetic and copies ran while one was open for 2% of the time, Pallas kernels for 9%

profile of v2, /device:TPU:86, one launch (start us, length us, event | category | flops | bytes accessed | tf_op | source)
XLA Modules:
  0.0 324.1 jit_solution(13974602993696473275)
XLA Ops:
  4.4 2.2 collective-permute-start
  9.8 20.4 %collective-permute-done.refs_1_ = bf16[264,2048]{1,0:T(8,128)(2,1)S(1)} collective-permute-done((bf16[264,2048]{1,0:T(8,128)(2,1)S(1)}, bf16[264,2048]{1,0:T(8,128)(2,1)S(1)}, u32[]{:S(2)}, u32[]{:S(2)}) %collective-permute-start) | collective-permute-done | bytes 1081376 | tf_op jit(solution)/shard_map/ppermute | solution.py:225
  31.2 10.6 %collective-permute-done.2.refs_2_ = bf16[264,2048]{1,0:T(8,128)(2,1)S(1)} collective-permute-done((bf16[264,2048]{1,0:T(8,128)(2,1)S(1)}, bf16[264,2048]{1,0:T(8,128)(2,1)S(1)}, u32[]{:S(2)}, u32[]{:S(2)}) %collective-permute-start.2) | collective-permute-done | bytes 1081376 | tf_op jit(solution)/shard_map/ppermute | solution.py:225
  42.8 10.6 %collective-permute-done.5.refs_0_ = bf16[264,2048]{1,0:T(8,128)(2,1)S(1)} collective-permute-done((bf16[264,2048]{1,0:T(8,128)(2,1)S(1)}, bf16[264,2048]{1,0:T(8,128)(2,1)S(1)}, u32[]{:S(2)}, u32[]{:S(2)}) %collective-permute-start.5) | collective-permute-done | bytes 1081376 | tf_op jit(solution)/shard_map/ppermute | solution.py:225
  54.4 10.6 %collective-permute-done.6.refs_1_ = bf16[264,2048]{1,0:T(8,128)(2,1)S(1)} collective-permute-done((bf16[264,2048]{1,0:T(8,128)(2,1)S(1)}, bf16[264,2048]{1,0:T(8,128)(2,1)S(1)}, u32[]{:S(2)}, u32[]{:S(2)}) %collective-permute-start.6) | collective-permute-done | bytes 1081376 | tf_op jit(solution)/shard_map/ppermute | solution.py:225
  65.9 10.6 %collective-permute-done.7.refs_2_ = bf16[264,2048]{1,0:T(8,128)(2,1)S(1)} collective-permute-done((bf16[264,2048]{1,0:T(8,128)(2,1)S(1)}, bf16[264,2048]{1,0:T(8,128)(2,1)S(1)}, u32[]{:S(2)}, u32[]{:S(2)}) %collective-permute-start.7) | collective-permute-done | bytes 1081376 | tf_op jit(solution)/shard_map/ppermute | solution.py:225
  77.6 10.6 %collective-permute-done.8.refs_3_ = bf16[264,2048]{1,0:T(8,128)(2,1)} collective-permute-done((bf16[264,2048]{1,0:T(8,128)(2,1)S(1)}, bf16[264,2048]{1,0:T(8,128)(2,1)}, u32[]{:S(2)}, u32[]{:S(2)}) %collective-permute-start.8) | collective-permute-done | bytes 1081376 | tf_op jit(solution)/shard_map/ppermute | solution.py:225
  88.3 11.4 %collective-permute-done.9.refs_0_.packet = bf16[264,2048]{1,0:T(8,128)(2,1)S(1)} collective-permute-done((bf16[264,2048]{1,0:T(8,128)(2,1)S(1)}, bf16[264,2048]{1,0:T(8,128)(2,1)S(1)}, u32[]{:S(2)}, u32[]{:S(2)}) %collective-permute-start.9) | collective-permute-done | bytes 1081376 | tf_op jit(solution)/shard_map/ppermute | solution.py:225
  99.7 2.5 compact.2
  102.2 9.1 %collective-permute-done.10.refs_1_.packet = bf16[264,2048]{1,0:T(8,128)(2,1)S(1)} collective-permute-done((bf16[264,2048]{1,0:T(8,128)(2,1)}, bf16[264,2048]{1,0:T(8,128)(2,1)S(1)}, u32[]{:S(2)}, u32[]{:S(2)}) %collective-permute-start.10) | collective-permute-done | bytes 1081376 | tf_op jit(solution)/shard_map/ppermute | solution.py:225
  111.3 2.5 compact.3
  113.8 7.7 %collective-permute-done.14.refs_0_ = bf16[232,2048]{1,0:T(8,128)(2,1)S(1)} collective-permute-done((bf16[232,2048]{1,0:T(8,128)(2,1)S(1)}, bf16[232,2048]{1,0:T(8,128)(2,1)S(1)}, u32[]{:S(2)}, u32[]{:S(2)}) %collective-permute-start.14) | collective-permute-done | bytes 950304 | tf_op jit(solution)/shard_map/ppermute | solution.py:225
  121.8 9.9 %collective-permute-done.15.refs_1_ = bf16[232,2048]{1,0:T(8,128)(2,1)S(1)} collective-permute-done((bf16[232,2048]{1,0:T(8,128)(2,1)S(1)}, bf16[232,2048]{1,0:T(8,128)(2,1)S(1)}, u32[]{:S(2)}, u32[]{:S(2)}) %collective-permute-start.15) | collective-permute-done | bytes 950304 | tf_op jit(solution)/shard_map/ppermute | solution.py:225
  131.9 7.1 %collective-permute-done.16.refs_2_ = bf16[168,2048]{1,0:T(8,128)(2,1)S(1)} collective-permute-done((bf16[168,2048]{1,0:T(8,128)(2,1)S(1)}, bf16[168,2048]{1,0:T(8,128)(2,1)S(1)}, u32[]{:S(2)}, u32[]{:S(2)}) %collective-permute-start.16) | collective-permute-done | bytes 688160 | tf_op jit(solution)/shard_map/ppermute | solution.py:225
  139.2 7.2 %collective-permute-done.17.refs_3_ = bf16[168,2048]{1,0:T(8,128)(2,1)S(1)} collective-permute-done((bf16[168,2048]{1,0:T(8,128)(2,1)S(1)}, bf16[168,2048]{1,0:T(8,128)(2,1)S(1)}, u32[]{:S(2)}, u32[]{:S(2)}) %collective-permute-start.17) | collective-permute-done | bytes 688160 | tf_op jit(solution)/shard_map/ppermute | solution.py:225
  146.6 4.4 %collective-permute-done.18.refs_0_ = bf16[104,2048]{1,0:T(8,128)(2,1)S(1)} collective-permute-done((bf16[104,2048]{1,0:T(8,128)(2,1)S(1)}, bf16[104,2048]{1,0:T(8,128)(2,1)S(1)}, u32[]{:S(2)}, u32[]{:S(2)}) %collective-permute-start.18) | collective-permute-done | bytes 426016 | tf_op jit(solution)/shard_map/ppermute | solution.py:225
  153.2 2.7 collective-permute-done.19.refs_1_
  159.7 4.7 %collective-permute-done.24.refs_1_ = bf16[40,2048]{1,0:T(8,128)(2,1)S(1)} collective-permute-done((bf16[40,2048]{1,0:T(8,128)(2,1)S(1)}, bf16[40,2048]{1,0:T(8,128)(2,1)S(1)}, u32[]{:S(2)}, u32[]{:S(2)}) %collective-permute-start.24) | collective-permute-done | bytes 163872 | tf_op jit(solution)/shard_map/ppermute | solution.py:225
  165.7 3.1 expert.7
  168.8 6.1 %expert.6 = (bf16[192,2048]{1,0:T(8,128)(2,1)S(1)}, bf16[192,2048]{1,0:T(8,128)(2,1)S(1)}) custom-call(bf16[128,2048]{1,0:T(8,128)(2,1)S(1)} %get-tuple-element.62.refs_0_, bf16[64,2048]{1,0:T(8,128)(2,1)S(1)} %get-tuple-element.63.refs_1_, bf16[128,2048]{1,0:T(8,128)(2,1)S(1)} %collective-permute-done.20.refs_2_, ...), custom_call_target="tpu_custom_call" | custom-call | flops 4831838208 | bytes 12582912 | tf_op jit(solution)/shard_map/expert/pallas_call | solution.py:195
  177.4 3.0 collective-permute-done.33
  180.7 2.2 collective-permute-start.34
  183.3 3.4 %select.26 = (bf16[128,2048]{1,0:T(8,128)(2,1)S(1)}, bf16[128,2048]{1,0:T(8,128)(2,1)S(1)}, bf16[128,256]{1,0:T(8,128)(2,1)S(1)}, bf16[128,256]{1,0:T(8,128)(2,1...) custom-call(s32[1]{0:T(128)} %bitcast.ids, f32[1,2048]{1,0:T(1,128)S(1)} %bitcast.33, ...), custom_call_target="tpu_custom_call" | custom-call | flops 301989888 | bytes 4325376 | tf_op jit(solution)/shard_map/select/pallas_call | solution.py:88
  190.3 3.4 %collective-permute-start.26 = (bf16[96,2048]{1,0:T(8,128)(2,1)S(1)}, bf16[96,2048]{1,0:T(8,128)(2,1)S(1)}, u32[]{:S(2)}, u32[]{:S(2)}) collective-permute-start(bf16[96,2048]{1,0:T(8,128)(2,1)S(1)} %fusion.12), channel_id=1, source_target_pairs={{0,30},{1,3},{2,0},{3,5},{4,2},{5,7},{6,4},{7,9},{8,6},{9,11},{10,... | collective-permute-start | bytes 1179656 | tf_op jit(solution)/shard_map/ppermute | solution.py:225
  194.2 6.1 %expert.5 = (bf16[192,2048]{1,0:T(8,128)(2,1)S(1)}, bf16[192,2048]{1,0:T(8,128)(2,1)S(1)}) custom-call(bf16[128,2048]{1,0:T(8,128)(2,1)S(1)} %get-tuple-element.50.refs_0_, bf16[64,2048]{1,0:T(8,128)(2,1)S(1)} %get-tuple-element.51.refs_1_, bf16[128,2048]{1,0:T(8,128)(2,1)S(1)} %collective-permute-done.11.refs_2_, ...), custom_call_target="tpu_custom_call" | custom-call | flops 4831838208 | bytes 12582912 | tf_op jit(solution)/shard_map/expert/pallas_call | solution.py:195
  200.9 2.3 collective-permute-start.27
  203.2 2.9 collective-permute-done.35
  206.5 4.0 %collective-permute-start.36 = (bf16[224,2048]{1,0:T(8,128)(2,1)S(1)}, bf16[224,2048]{1,0:T(8,128)(2,1)S(1)}, u32[]{:S(2)}, u32[]{:S(2)}) collective-permute-start(bf16[224,2048]{1,0:T(8,128)(2,1)S(1)} %fusion.9), channel_id=1, source_target_pairs={{0,30},{1,3},{2,0},{3,5},{4,2},{5,7},{6,4},{7,9},{8,6},{9,11},{10,... | collective-permute-start | bytes 2752520 | tf_op jit(solution)/shard_map/ppermute | solution.py:225
  210.6 2.4 collective-permute-done.27
  213.5 3.8 %collective-permute-start.28 = (bf16[224,2048]{1,0:T(8,128)(2,1)S(1)}, bf16[224,2048]{1,0:T(8,128)(2,1)S(1)}, u32[]{:S(2)}, u32[]{:S(2)}) collective-permute-start(bf16[224,2048]{1,0:T(8,128)(2,1)S(1)} %fusion.8), channel_id=1, source_target_pairs={{0,30},{1,3},{2,0},{3,5},{4,2},{5,7},{6,4},{7,9},{8,6},{9,11},{10,... | collective-permute-start | bytes 2752520 | tf_op jit(solution)/shard_map/ppermute | solution.py:225
  217.3 5.6 %collective-permute-done.36 = bf16[224,2048]{1,0:T(8,128)(2,1)S(1)} collective-permute-done((bf16[224,2048]{1,0:T(8,128)(2,1)S(1)}, bf16[224,2048]{1,0:T(8,128)(2,1)S(1)}, u32[]{:S(2)}, u32[]{:S(2)}) %collective-permute-start.36) | collective-permute-done | bytes 917536 | tf_op jit(solution)/shard_map/ppermute | solution.py:225
  223.8 3.8 %collective-permute-start.37 = (bf16[256,2048]{1,0:T(8,128)(2,1)S(1)}, bf16[256,2048]{1,0:T(8,128)(2,1)S(1)}, u32[]{:S(2)}, u32[]{:S(2)}) collective-permute-start(bf16[256,2048]{1,0:T(8,128)(2,1)S(1)} %fusion.7), channel_id=1, source_target_pairs={{0,30},{1,3},{2,0},{3,5},{4,2},{5,7},{6,4},{7,9},{8,6},{9,11},{10,... | collective-permute-start | bytes 3145736 | tf_op jit(solution)/shard_map/ppermute | solution.py:225
  227.6 5.1 %collective-permute-done.28 = bf16[224,2048]{1,0:T(8,128)(2,1)S(1)} collective-permute-done((bf16[224,2048]{1,0:T(8,128)(2,1)S(1)}, bf16[224,2048]{1,0:T(8,128)(2,1)S(1)}, u32[]{:S(2)}, u32[]{:S(2)}) %collective-permute-start.28) | collective-permute-done | bytes 917536 | tf_op jit(solution)/shard_map/ppermute | solution.py:225
  233.7 3.8 %collective-permute-start.29 = (bf16[256,2048]{1,0:T(8,128)(2,1)S(1)}, bf16[256,2048]{1,0:T(8,128)(2,1)S(1)}, u32[]{:S(2)}, u32[]{:S(2)}) collective-permute-start(bf16[256,2048]{1,0:T(8,128)(2,1)S(1)} %fusion.3), channel_id=1, source_target_pairs={{0,30},{1,3},{2,0},{3,5},{4,2},{5,7},{6,4},{7,9},{8,6},{9,11},{10,... | collective-permute-start | bytes 3145736 | tf_op jit(solution)/shard_map/ppermute | solution.py:225
  237.5 6.5 %collective-permute-done.37 = bf16[256,2048]{1,0:T(8,128)(2,1)S(1)} collective-permute-done((bf16[256,2048]{1,0:T(8,128)(2,1)S(1)}, bf16[256,2048]{1,0:T(8,128)(2,1)S(1)}, u32[]{:S(2)}, u32[]{:S(2)}) %collective-permute-start.37) | collective-permute-done | bytes 1048608 | tf_op jit(solution)/shard_map/ppermute | solution.py:225
  244.4 3.8 %collective-permute-start.38 = (bf16[256,2048]{1,0:T(8,128)(2,1)S(1)}, bf16[256,2048]{1,0:T(8,128)(2,1)S(1)}, u32[]{:S(2)}, u32[]{:S(2)}) collective-permute-start(bf16[256,2048]{1,0:T(8,128)(2,1)S(1)} %fusion.6), channel_id=1, source_target_pairs={{0,30},{1,3},{2,0},{3,5},{4,2},{5,7},{6,4},{7,9},{8,6},{9,11},{10,... | collective-permute-start | bytes 3145736 | tf_op jit(solution)/shard_map/ppermute | solution.py:225
  252.0 3.8 %expert.4 = (bf16[96,2048]{1,0:T(8,128)(2,1)S(1)}, bf16[96,2048]{1,0:T(8,128)(2,1)S(1)}) custom-call(bf16[96,2048]{1,0:T(8,128)(2,1)S(1)} %get-tuple-element.44.refs_0_, bf16[96,2048]{1,0:T(8,128)(2,1)S(1)} %collective-permute-done.3.refs_1_, bf16[1,2048,1024]{2,1,0:T(8,128)(2,1)S(1)} %copy-done, bf16[1,2048,1024]{2,1,0:T(8,128)(2,1)S(1)} %copy-done.1, ...), custom_call_target="tpu_custom_call" | custom-call | flops 2415919104 | bytes 12582912 | tf_op jit(solution)/shard_map/expert/pallas_call | solution.py:195
  256.5 2.9 collective-permute-start.30
  259.5 7.0 %collective-permute-done.38 = bf16[256,2048]{1,0:T(8,128)(2,1)S(1)} collective-permute-done((bf16[256,2048]{1,0:T(8,128)(2,1)S(1)}, bf16[256,2048]{1,0:T(8,128)(2,1)S(1)}, u32[]{:S(2)}, u32[]{:S(2)}) %collective-permute-start.38) | collective-permute-done | bytes 1048608 | tf_op jit(solution)/shard_map/ppermute | solution.py:225
  266.9 3.8 %collective-permute-start.39 = (bf16[256,2048]{1,0:T(8,128)(2,1)S(1)}, bf16[256,2048]{1,0:T(8,128)(2,1)S(1)}, u32[]{:S(2)}, u32[]{:S(2)}) collective-permute-start(bf16[256,2048]{1,0:T(8,128)(2,1)S(1)} %fusion.5), channel_id=1, source_target_pairs={{0,30},{1,3},{2,0},{3,5},{4,2},{5,7},{6,4},{7,9},{8,6},{9,11},{10,... | collective-permute-start | bytes 3145736 | tf_op jit(solution)/shard_map/ppermute | solution.py:225
  270.8 6.9 %collective-permute-done.30 = bf16[256,2048]{1,0:T(8,128)(2,1)S(1)} collective-permute-done((bf16[256,2048]{1,0:T(8,128)(2,1)S(1)}, bf16[256,2048]{1,0:T(8,128)(2,1)S(1)}, u32[]{:S(2)}, u32[]{:S(2)}) %collective-permute-start.30) | collective-permute-done | bytes 1048608 | tf_op jit(solution)/shard_map/ppermute | solution.py:225
  278.1 3.8 %collective-permute-start.31 = (bf16[256,2048]{1,0:T(8,128)(2,1)S(1)}, bf16[256,2048]{1,0:T(8,128)(2,1)S(1)}, u32[]{:S(2)}, u32[]{:S(2)}) collective-permute-start(bf16[256,2048]{1,0:T(8,128)(2,1)S(1)} %fusion.1), channel_id=1, source_target_pairs={{0,30},{1,3},{2,0},{3,5},{4,2},{5,7},{6,4},{7,9},{8,6},{9,11},{10,... | collective-permute-start | bytes 3145736 | tf_op jit(solution)/shard_map/ppermute | solution.py:225
  281.9 7.0 %collective-permute-done.39 = bf16[256,2048]{1,0:T(8,128)(2,1)S(1)} collective-permute-done((bf16[256,2048]{1,0:T(8,128)(2,1)S(1)}, bf16[256,2048]{1,0:T(8,128)(2,1)S(1)}, u32[]{:S(2)}, u32[]{:S(2)}) %collective-permute-start.39) | collective-permute-done | bytes 1048608 | tf_op jit(solution)/shard_map/ppermute | solution.py:225
  289.4 3.8 %collective-permute-start.40 = (bf16[256,2048]{1,0:T(8,128)(2,1)S(1)}, bf16[256,2048]{1,0:T(8,128)(2,1)S(1)}, u32[]{:S(2)}, u32[]{:S(2)}) collective-permute-start(bf16[256,2048]{1,0:T(8,128)(2,1)S(1)} %fusion.4), channel_id=1, source_target_pairs={{0,30},{1,3},{2,0},{3,5},{4,2},{5,7},{6,4},{7,9},{8,6},{9,11},{10,... | collective-permute-start | bytes 3145736 | tf_op jit(solution)/shard_map/ppermute | solution.py:225
  293.2 7.0 %collective-permute-done.31 = bf16[256,2048]{1,0:T(8,128)(2,1)S(1)} collective-permute-done((bf16[256,2048]{1,0:T(8,128)(2,1)S(1)}, bf16[256,2048]{1,0:T(8,128)(2,1)S(1)}, u32[]{:S(2)}, u32[]{:S(2)}) %collective-permute-start.31) | collective-permute-done | bytes 1048608 | tf_op jit(solution)/shard_map/ppermute | solution.py:225
  300.6 3.8 %collective-permute-start.32 = (bf16[256,2048]{1,0:T(8,128)(2,1)S(1)}, bf16[256,2048]{1,0:T(8,128)(2,1)S(1)}, u32[]{:S(2)}, u32[]{:S(2)}) collective-permute-start(bf16[256,2048]{1,0:T(8,128)(2,1)S(1)} %fusion), channel_id=1, source_target_pairs={{0,30},{1,3},{2,0},{3,5},{4,2},{5,7},{6,4},{7,9},{8,6},{9,11},{10,... | collective-permute-start | bytes 3145736 | tf_op jit(solution)/shard_map/ppermute | solution.py:225
  304.4 7.0 %collective-permute-done.40 = bf16[256,2048]{1,0:T(8,128)(2,1)S(1)} collective-permute-done((bf16[256,2048]{1,0:T(8,128)(2,1)S(1)}, bf16[256,2048]{1,0:T(8,128)(2,1)S(1)}, u32[]{:S(2)}, u32[]{:S(2)}) %collective-permute-start.40) | collective-permute-done | bytes 1048608 | tf_op jit(solution)/shard_map/ppermute | solution.py:225
  311.4 11.2 %collective-permute-done.32 = bf16[256,2048]{1,0:T(8,128)(2,1)S(1)} collective-permute-done((bf16[256,2048]{1,0:T(8,128)(2,1)S(1)}, bf16[256,2048]{1,0:T(8,128)(2,1)S(1)}, u32[]{:S(2)}, u32[]{:S(2)}) %collective-permute-start.32) | collective-permute-done | bytes 1048608 | tf_op jit(solution)/shard_map/ppermute | solution.py:225
  (140 shorter events, 39.6 us)
Async XLA Ops:
  4.3 3.4 %collective-permute-start.1 = (bf16[264,2048]{1,0:T(8,128)(2,1)S(1)}, bf16[264,2048]{1,0:T(8,128)(2,1)S(1)}, u32[]{:S(2)}, u32[]{:S(2)}) collective-permute-start(bf16[264,2048]{1,0:T(8,128)(2,1)S(1)} %fusion.15.refs_0_), channel_id=1, source_target_pairs={{0,1},{1,0},{2,3},{3,2},{4,5},{5,4},{6,7},{7,6},{8,9},{9,8},{10,11... | collective-permute-start | bytes 3244040 | tf_op jit(solution)/shard_map/ppermute | solution.py:232
  4.4 25.8 %collective-permute-start = (bf16[264,2048]{1,0:T(8,128)(2,1)S(1)}, bf16[264,2048]{1,0:T(8,128)(2,1)S(1)}, u32[]{:S(2)}, u32[]{:S(2)}) collective-permute-start(bf16[264,2048]{1,0:T(8,128)(2,1)S(1)} %fusion.15.refs_0_), channel_id=1, source_target_pairs={{0,2},{1,31},{2,4},{3,1},{4,6},{5,3},{6,8},{7,5},{8,10},{9,7},{10,... | collective-permute-start | bytes 3244040 | tf_op jit(solution)/shard_map/ppermute | solution.py:225
  7.7 34.1 %collective-permute-start.2 = (bf16[264,2048]{1,0:T(8,128)(2,1)S(1)}, bf16[264,2048]{1,0:T(8,128)(2,1)S(1)}, u32[]{:S(2)}, u32[]{:S(2)}) collective-permute-start(bf16[264,2048]{1,0:T(8,128)(2,1)S(1)} %collective-permute-done.1), channel_id=1, source_target_pairs={{0,2},{1,31},{2,4},{3,1},{4,6},{5,3},{6,8},{7,5},{8,10},{9,7},{10,... | collective-permute-start | bytes 3244040 | tf_op jit(solution)/shard_map/ppermute | solution.py:225
  30.2 23.2 %collective-permute-start.5 = (bf16[264,2048]{1,0:T(8,128)(2,1)S(1)}, bf16[264,2048]{1,0:T(8,128)(2,1)S(1)}, u32[]{:S(2)}, u32[]{:S(2)}) collective-permute-start(bf16[264,2048]{1,0:T(8,128)(2,1)S(1)} %collective-permute-done.refs_1_), channel_id=1, source_target_pairs={{0,2},{1,31},{2,4},{3,1},{4,6},{5,3},{6,8},{7,5},{8,10},{9,7},{10,... | collective-permute-start | bytes 3244040 | tf_op jit(solution)/shard_map/ppermute | solution.py:225
  41.8 23.2 %collective-permute-start.6 = (bf16[264,2048]{1,0:T(8,128)(2,1)S(1)}, bf16[264,2048]{1,0:T(8,128)(2,1)S(1)}, u32[]{:S(2)}, u32[]{:S(2)}) collective-permute-start(bf16[264,2048]{1,0:T(8,128)(2,1)S(1)} %collective-permute-done.2.refs_2_), channel_id=1, source_target_pairs={{0,2},{1,31},{2,4},{3,1},{4,6},{5,3},{6,8},{7,5},{8,10},{9,7},{10,... | collective-permute-start | bytes 3244040 | tf_op jit(solution)/shard_map/ppermute | solution.py:225
  53.4 23.2 %collective-permute-start.7 = (bf16[264,2048]{1,0:T(8,128)(2,1)S(1)}, bf16[264,2048]{1,0:T(8,128)(2,1)S(1)}, u32[]{:S(2)}, u32[]{:S(2)}) collective-permute-start(bf16[264,2048]{1,0:T(8,128)(2,1)S(1)} %collective-permute-done.5.refs_0_), channel_id=1, source_target_pairs={{0,2},{1,31},{2,4},{3,1},{4,6},{5,3},{6,8},{7,5},{8,10},{9,7},{10,... | collective-permute-start | bytes 3244040 | tf_op jit(solution)/shard_map/ppermute | solution.py:225
  64.9 23.3 %collective-permute-start.8 = (bf16[264,2048]{1,0:T(8,128)(2,1)S(1)}, bf16[264,2048]{1,0:T(8,128)(2,1)}, u32[]{:S(2)}, u32[]{:S(2)}) collective-permute-start(bf16[264,2048]{1,0:T(8,128)(2,1)S(1)} %collective-permute-done.6.refs_1_), channel_id=1, source_target_pairs={{0,2},{1,31},{2,4},{3,1},{4,6},{5,3},{6,8},{7,5},{8,10},{9,7},{10,... | collective-permute-start | bytes 3244040 | tf_op jit(solution)/shard_map/ppermute | solution.py:225
  76.5 23.2 %collective-permute-start.9 = (bf16[264,2048]{1,0:T(8,128)(2,1)S(1)}, bf16[264,2048]{1,0:T(8,128)(2,1)S(1)}, u32[]{:S(2)}, u32[]{:S(2)}) collective-permute-start(bf16[264,2048]{1,0:T(8,128)(2,1)S(1)} %collective-permute-done.7.refs_2_), channel_id=1, source_target_pairs={{0,2},{1,31},{2,4},{3,1},{4,6},{5,3},{6,8},{7,5},{8,10},{9,7},{10,... | collective-permute-start | bytes 3244040 | tf_op jit(solution)/shard_map/ppermute | solution.py:225
  88.2 23.1 %collective-permute-start.10 = (bf16[264,2048]{1,0:T(8,128)(2,1)}, bf16[264,2048]{1,0:T(8,128)(2,1)S(1)}, u32[]{:S(2)}, u32[]{:S(2)}) collective-permute-start(bf16[264,2048]{1,0:T(8,128)(2,1)} %collective-permute-done.8.refs_3_), channel_id=1, source_target_pairs={{0,2},{1,31},{2,4},{3,1},{4,6},{5,3},{6,8},{7,5},{8,10},{9,7},{10,... | collective-permute-start | bytes 3244040 | tf_op jit(solution)/shard_map/ppermute | solution.py:225
  99.7 21.8 %copy-start.3 = (bf16[264,2048]{1,0:T(8,128)(2,1)}, bf16[264,2048]{1,0:T(8,128)(2,1)S(1)}, u32[]{:S(2)}) copy-start(bf16[264,2048]{1,0:T(8,128)(2,1)S(1)} %collective-permute-done.9.refs_0_.packet) | copy-start | bytes 3244036
  102.2 19.3 %collective-permute-start.14 = (bf16[232,2048]{1,0:T(8,128)(2,1)S(1)}, bf16[232,2048]{1,0:T(8,128)(2,1)S(1)}, u32[]{:S(2)}, u32[]{:S(2)}) collective-permute-start(bf16[232,2048]{1,0:T(8,128)(2,1)S(1)} %get-tuple-element.59), channel_id=1, source_target_pairs={{0,2},{1,31},{2,4},{3,1},{4,6},{5,3},{6,8},{7,5},{8,10},{9,7},{10,... | collective-permute-start | bytes 2850824 | tf_op jit(solution)/shard_map/ppermute | solution.py:225
  113.8 17.9 %collective-permute-start.15 = (bf16[232,2048]{1,0:T(8,128)(2,1)S(1)}, bf16[232,2048]{1,0:T(8,128)(2,1)S(1)}, u32[]{:S(2)}, u32[]{:S(2)}) collective-permute-start(bf16[232,2048]{1,0:T(8,128)(2,1)S(1)} %get-tuple-element.60), channel_id=1, source_target_pairs={{0,2},{1,31},{2,4},{3,1},{4,6},{5,3},{6,8},{7,5},{8,10},{9,7},{10,... | collective-permute-start | bytes 2850824 | tf_op jit(solution)/shard_map/ppermute | solution.py:225
  121.5 44.1 %copy-start.2 = (bf16[1,1024,2048]{2,1,0:T(8,128)(2,1)S(1)}, bf16[1,1024,2048]{2,1,0:T(8,128)(2,1)}, u32[]{:S(2)}) copy-start(bf16[1,1024,2048]{2,1,0:T(8,128)(2,1)} %refs_3_.3) | copy-start | bytes 12582916
  121.6 17.4 %collective-permute-start.16 = (bf16[168,2048]{1,0:T(8,128)(2,1)S(1)}, bf16[168,2048]{1,0:T(8,128)(2,1)S(1)}, u32[]{:S(2)}, u32[]{:S(2)}) collective-permute-start(bf16[168,2048]{1,0:T(8,128)(2,1)S(1)} %pad_maximum_fusion), channel_id=1, source_target_pairs={{0,2},{1,31},{2,4},{3,1},{4,6},{5,3},{6,8},{7,5},{8,10},{9,7},{10,... | collective-permute-start | bytes 2064392 | tf_op jit(solution)/shard_map/ppermute | solution.py:225
  131.8 19.2 %copy-start.19 = (f32[2048]{0:T(1024)S(1)}, f32[2048]{0:T(1024)}, u32[]{:S(2)}) copy-start(f32[2048]{0:T(1024)} %param.8) | copy-start | bytes 24580
  131.8 14.6 %collective-permute-start.17 = (bf16[168,2048]{1,0:T(8,128)(2,1)S(1)}, bf16[168,2048]{1,0:T(8,128)(2,1)S(1)}, u32[]{:S(2)}, u32[]{:S(2)}) collective-permute-start(bf16[168,2048]{1,0:T(8,128)(2,1)S(1)} %pad_maximum_fusion.1), channel_id=1, source_target_pairs={{0,2},{1,31},{2,4},{3,1},{4,6},{5,3},{6,8},{7,5},{8,10},{9,7},{10,... | collective-permute-start | bytes 2064392 | tf_op jit(solution)/shard_map/ppermute | solution.py:225
  139.0 26.7 %copy-start.1 = (bf16[1,2048,1024]{2,1,0:T(8,128)(2,1)S(1)}, bf16[1,2048,1024]{2,1,0:T(8,128)(2,1)}, u32[]{:S(2)}) copy-start(bf16[1,2048,1024]{2,1,0:T(8,128)(2,1)} %refs_2_.3) | copy-start | bytes 12582916
  139.1 11.9 %collective-permute-start.18 = (bf16[104,2048]{1,0:T(8,128)(2,1)S(1)}, bf16[104,2048]{1,0:T(8,128)(2,1)S(1)}, u32[]{:S(2)}, u32[]{:S(2)}) collective-permute-start(bf16[104,2048]{1,0:T(8,128)(2,1)S(1)} %pad_maximum_fusion.2), channel_id=1, source_target_pairs={{0,2},{1,31},{2,4},{3,1},{4,6},{5,3},{6,8},{7,5},{8,10},{9,7},{10,... | collective-permute-start | bytes 1277960 | tf_op jit(solution)/shard_map/ppermute | solution.py:225
  146.5 9.4 %collective-permute-start.19 = (bf16[104,2048]{1,0:T(8,128)(2,1)S(1)}, bf16[104,2048]{1,0:T(8,128)(2,1)S(1)}, u32[]{:S(2)}, u32[]{:S(2)}) collective-permute-start(bf16[104,2048]{1,0:T(8,128)(2,1)S(1)} %pad_maximum_fusion.3), channel_id=1, source_target_pairs={{0,2},{1,31},{2,4},{3,1},{4,6},{5,3},{6,8},{7,5},{8,10},{9,7},{10,... | collective-permute-start | bytes 1277960 | tf_op jit(solution)/shard_map/ppermute | solution.py:225
  151.0 14.7 %copy-start = (bf16[1,2048,1024]{2,1,0:T(8,128)(2,1)S(1)}, bf16[1,2048,1024]{2,1,0:T(8,128)(2,1)}, u32[]{:S(2)}) copy-start(bf16[1,2048,1024]{2,1,0:T(8,128)(2,1)} %refs_1_.1) | copy-start | bytes 12582916
  152.9 15.9 %collective-permute-start.20 = (bf16[128,2048]{1,0:T(8,128)(2,1)S(1)}, bf16[128,2048]{1,0:T(8,128)(2,1)S(1)}, u32[]{:S(2)}, u32[]{:S(2)}) collective-permute-start(bf16[128,2048]{1,0:T(8,128)(2,1)S(1)} %get-tuple-element.64), channel_id=1, source_target_pairs={{0,1},{1,0},{2,3},{3,2},{4,5},{5,4},{6,7},{7,6},{8,9},{9,8},{10,11... | collective-permute-start | bytes 1572872 | tf_op jit(solution)/shard_map/ppermute | solution.py:232
  153.1 6.6 %collective-permute-start.23 = (bf16[40,2048]{1,0:T(8,128)(2,1)S(1)}, bf16[40,2048]{1,0:T(8,128)(2,1)S(1)}, u32[]{:S(2)}, u32[]{:S(2)}) collective-permute-start(bf16[40,2048]{1,0:T(8,128)(2,1)S(1)} %pad_maximum_fusion.4), channel_id=1, source_target_pairs={{0,2},{1,31},{2,4},{3,1},{4,6},{5,3},{6,8},{7,5},{8,10},{9,7},{10,... | collective-permute-start | bytes 491528 | tf_op jit(solution)/shard_map/ppermute | solution.py:225
  157.4 11.4 %collective-permute-start.21 = (bf16[64,2048]{1,0:T(8,128)(2,1)S(1)}, bf16[64,2048]{1,0:T(8,128)(2,1)S(1)}, u32[]{:S(2)}, u32[]{:S(2)}) collective-permute-start(bf16[64,2048]{1,0:T(8,128)(2,1)S(1)} %get-tuple-element.65), channel_id=1, source_target_pairs={{0,1},{1,0},{2,3},{3,2},{4,5},{5,4},{6,7},{7,6},{8,9},{9,8},{10,11... | collective-permute-start | bytes 786440 | tf_op jit(solution)/shard_map/ppermute | solution.py:232
  157.6 6.8 %collective-permute-start.24 = (bf16[40,2048]{1,0:T(8,128)(2,1)S(1)}, bf16[40,2048]{1,0:T(8,128)(2,1)S(1)}, u32[]{:S(2)}, u32[]{:S(2)}) collective-permute-start(bf16[40,2048]{1,0:T(8,128)(2,1)S(1)} %pad_maximum_fusion.5), channel_id=1, source_target_pairs={{0,2},{1,31},{2,4},{3,1},{4,6},{5,3},{6,8},{7,5},{8,10},{9,7},{10,... | collective-permute-start | bytes 491528 | tf_op jit(solution)/shard_map/ppermute | solution.py:225
  175.0 2.4 collective-permute-start.22
  175.3 5.1 %collective-permute-start.33 = (bf16[32,2048]{1,0:T(8,128)(2,1)S(1)}, bf16[32,2048]{1,0:T(8,128)(2,1)S(1)}, u32[]{:S(2)}, u32[]{:S(2)}) collective-permute-start(bf16[32,2048]{1,0:T(8,128)(2,1)S(1)} %convolution_convert_fusion), channel_id=1, source_target_pairs={{0,30},{1,3},{2,0},{3,5},{4,2},{5,7},{6,4},{7,9},{8,6},{9,11},{10,... | collective-permute-start | bytes 393224 | tf_op jit(solution)/shard_map/ppermute | solution.py:225
  180.7 13.0 %collective-permute-start.34 = (bf16[96,2048]{1,0:T(8,128)(2,1)S(1)}, bf16[96,2048]{1,0:T(8,128)(2,1)S(1)}, u32[]{:S(2)}, u32[]{:S(2)}) collective-permute-start(bf16[96,2048]{1,0:T(8,128)(2,1)S(1)} %fusion.13), channel_id=1, source_target_pairs={{0,30},{1,3},{2,0},{3,5},{4,2},{5,7},{6,4},{7,9},{8,6},{9,11},{10,... | collective-permute-start | bytes 1179656 | tf_op jit(solution)/shard_map/ppermute | solution.py:225
  183.2 6.8 %collective-permute-start.25 = (bf16[32,2048]{1,0:T(8,128)(2,1)S(1)}, bf16[32,2048]{1,0:T(8,128)(2,1)S(1)}, u32[]{:S(2)}, u32[]{:S(2)}) collective-permute-start(bf16[32,2048]{1,0:T(8,128)(2,1)S(1)} %convolution_convert_fusion.1), channel_id=1, source_target_pairs={{0,30},{1,3},{2,0},{3,5},{4,2},{5,7},{6,4},{7,9},{8,6},{9,11},{10,... | collective-permute-start | bytes 393224 | tf_op jit(solution)/shard_map/ppermute | solution.py:225
  186.7 7.5 %collective-permute-start.11 = (bf16[128,2048]{1,0:T(8,128)(2,1)S(1)}, bf16[128,2048]{1,0:T(8,128)(2,1)S(1)}, u32[]{:S(2)}, u32[]{:S(2)}) collective-permute-start(bf16[128,2048]{1,0:T(8,128)(2,1)S(1)} %get-tuple-element.52), channel_id=1, source_target_pairs={{0,1},{1,0},{2,3},{3,2},{4,5},{5,4},{6,7},{7,6},{8,9},{9,8},{10,11... | collective-permute-start | bytes 1572872 | tf_op jit(solution)/shard_map/ppermute | solution.py:232
  188.6 5.7 %collective-permute-start.12 = (bf16[64,2048]{1,0:T(8,128)(2,1)S(1)}, bf16[64,2048]{1,0:T(8,128)(2,1)S(1)}, u32[]{:S(2)}, u32[]{:S(2)}) collective-permute-start(bf16[64,2048]{1,0:T(8,128)(2,1)S(1)} %get-tuple-element.53), channel_id=1, source_target_pairs={{0,1},{1,0},{2,3},{3,2},{4,5},{5,4},{6,7},{7,6},{8,9},{9,8},{10,11... | collective-permute-start | bytes 786440 | tf_op jit(solution)/shard_map/ppermute | solution.py:232
  190.3 10.2 %collective-permute-start.26 = (bf16[96,2048]{1,0:T(8,128)(2,1)S(1)}, bf16[96,2048]{1,0:T(8,128)(2,1)S(1)}, u32[]{:S(2)}, u32[]{:S(2)}) collective-permute-start(bf16[96,2048]{1,0:T(8,128)(2,1)S(1)} %fusion.12), channel_id=1, source_target_pairs={{0,30},{1,3},{2,0},{3,5},{4,2},{5,7},{6,4},{7,9},{8,6},{9,11},{10,... | collective-permute-start | bytes 1179656 | tf_op jit(solution)/shard_map/ppermute | solution.py:225
  194.1 12.0 %collective-permute-start.35 = (bf16[160,2048]{1,0:T(8,128)(2,1)S(1)}, bf16[160,2048]{1,0:T(8,128)(2,1)S(1)}, u32[]{:S(2)}, u32[]{:S(2)}) collective-permute-start(bf16[160,2048]{1,0:T(8,128)(2,1)S(1)} %fusion.11), channel_id=1, source_target_pairs={{0,30},{1,3},{2,0},{3,5},{4,2},{5,7},{6,4},{7,9},{8,6},{9,11},{10,... | collective-permute-start | bytes 1966088 | tf_op jit(solution)/shard_map/ppermute | solution.py:225
  200.4 10.2 %collective-permute-start.13 = (bf16[192,2048]{1,0:T(8,128)(2,1)S(1)}, bf16[192,2048]{1,0:T(8,128)(2,1)S(1)}, u32[]{:S(2)}, u32[]{:S(2)}) collective-permute-start(bf16[192,2048]{1,0:T(8,128)(2,1)S(1)} %get-tuple-element.55), channel_id=1, source_target_pairs={{0,1},{1,0},{2,3},{3,2},{4,5},{5,4},{6,7},{7,6},{8,9},{9,8},{10,11... | collective-permute-start | bytes 2359304 | tf_op jit(solution)/shard_map/ppermute | solution.py:232
  200.9 12.2 %collective-permute-start.27 = (bf16[160,2048]{1,0:T(8,128)(2,1)S(1)}, bf16[160,2048]{1,0:T(8,128)(2,1)S(1)}, u32[]{:S(2)}, u32[]{:S(2)}) collective-permute-start(bf16[160,2048]{1,0:T(8,128)(2,1)S(1)} %fusion.10), channel_id=1, source_target_pairs={{0,30},{1,3},{2,0},{3,5},{4,2},{5,7},{6,4},{7,9},{8,6},{9,11},{10,... | collective-permute-start | bytes 1966088 | tf_op jit(solution)/shard_map/ppermute | solution.py:225
  206.5 16.4 %collective-permute-start.36 = (bf16[224,2048]{1,0:T(8,128)(2,1)S(1)}, bf16[224,2048]{1,0:T(8,128)(2,1)S(1)}, u32[]{:S(2)}, u32[]{:S(2)}) collective-permute-start(bf16[224,2048]{1,0:T(8,128)(2,1)S(1)} %fusion.9), channel_id=1, source_target_pairs={{0,30},{1,3},{2,0},{3,5},{4,2},{5,7},{6,4},{7,9},{8,6},{9,11},{10,... | collective-permute-start | bytes 2752520 | tf_op jit(solution)/shard_map/ppermute | solution.py:225
  213.5 19.2 %collective-permute-start.28 = (bf16[224,2048]{1,0:T(8,128)(2,1)S(1)}, bf16[224,2048]{1,0:T(8,128)(2,1)S(1)}, u32[]{:S(2)}, u32[]{:S(2)}) collective-permute-start(bf16[224,2048]{1,0:T(8,128)(2,1)S(1)} %fusion.8), channel_id=1, source_target_pairs={{0,30},{1,3},{2,0},{3,5},{4,2},{5,7},{6,4},{7,9},{8,6},{9,11},{10,... | collective-permute-start | bytes 2752520 | tf_op jit(solution)/shard_map/ppermute | solution.py:225
  223.8 20.1 %collective-permute-start.37 = (bf16[256,2048]{1,0:T(8,128)(2,1)S(1)}, bf16[256,2048]{1,0:T(8,128)(2,1)S(1)}, u32[]{:S(2)}, u32[]{:S(2)}) collective-permute-start(bf16[256,2048]{1,0:T(8,128)(2,1)S(1)} %fusion.7), channel_id=1, source_target_pairs={{0,30},{1,3},{2,0},{3,5},{4,2},{5,7},{6,4},{7,9},{8,6},{9,11},{10,... | collective-permute-start | bytes 3145736 | tf_op jit(solution)/shard_map/ppermute | solution.py:225
  233.2 15.0 %copy-start.18 = (bf16[264,2048]{1,0:T(8,128)(2,1)S(1)}, bf16[264,2048]{1,0:T(8,128)(2,1)}, u32[]{:S(2)}) copy-start(bf16[264,2048]{1,0:T(8,128)(2,1)} %copy-done.17) | copy-start | bytes 3244036
  233.7 22.4 %collective-permute-start.29 = (bf16[256,2048]{1,0:T(8,128)(2,1)S(1)}, bf16[256,2048]{1,0:T(8,128)(2,1)S(1)}, u32[]{:S(2)}, u32[]{:S(2)}) collective-permute-start(bf16[256,2048]{1,0:T(8,128)(2,1)S(1)} %fusion.3), channel_id=1, source_target_pairs={{0,30},{1,3},{2,0},{3,5},{4,2},{5,7},{6,4},{7,9},{8,6},{9,11},{10,... | collective-permute-start | bytes 3145736 | tf_op jit(solution)/shard_map/ppermute | solution.py:225
  244.4 22.0 %collective-permute-start.38 = (bf16[256,2048]{1,0:T(8,128)(2,1)S(1)}, bf16[256,2048]{1,0:T(8,128)(2,1)S(1)}, u32[]{:S(2)}, u32[]{:S(2)}) collective-permute-start(bf16[256,2048]{1,0:T(8,128)(2,1)S(1)} %fusion.6), channel_id=1, source_target_pairs={{0,30},{1,3},{2,0},{3,5},{4,2},{5,7},{6,4},{7,9},{8,6},{9,11},{10,... | collective-permute-start | bytes 3145736 | tf_op jit(solution)/shard_map/ppermute | solution.py:225
  250.2 1.8 collective-permute-start.3
  255.8 14.9 %collective-permute-start.4 = (bf16[96,2048]{1,0:T(8,128)(2,1)S(1)}, bf16[96,2048]{1,0:T(8,128)(2,1)S(1)}, u32[]{:S(2)}, u32[]{:S(2)}) collective-permute-start(bf16[96,2048]{1,0:T(8,128)(2,1)S(1)} %get-tuple-element.47), channel_id=1, source_target_pairs={{0,1},{1,0},{2,3},{3,2},{4,5},{5,4},{6,7},{7,6},{8,9},{9,8},{10,11... | collective-permute-start | bytes 1179656 | tf_op jit(solution)/shard_map/ppermute | solution.py:232
  256.5 21.1 %collective-permute-start.30 = (bf16[256,2048]{1,0:T(8,128)(2,1)S(1)}, bf16[256,2048]{1,0:T(8,128)(2,1)S(1)}, u32[]{:S(2)}, u32[]{:S(2)}) collective-permute-start(bf16[256,2048]{1,0:T(8,128)(2,1)S(1)} %fusion.2), channel_id=1, source_target_pairs={{0,30},{1,3},{2,0},{3,5},{4,2},{5,7},{6,4},{7,9},{8,6},{9,11},{10,... | collective-permute-start | bytes 3145736 | tf_op jit(solution)/shard_map/ppermute | solution.py:225
  266.9 22.0 %collective-permute-start.39 = (bf16[256,2048]{1,0:T(8,128)(2,1)S(1)}, bf16[256,2048]{1,0:T(8,128)(2,1)S(1)}, u32[]{:S(2)}, u32[]{:S(2)}) collective-permute-start(bf16[256,2048]{1,0:T(8,128)(2,1)S(1)} %fusion.5), channel_id=1, source_target_pairs={{0,30},{1,3},{2,0},{3,5},{4,2},{5,7},{6,4},{7,9},{8,6},{9,11},{10,... | collective-permute-start | bytes 3145736 | tf_op jit(solution)/shard_map/ppermute | solution.py:225
  278.1 22.0 %collective-permute-start.31 = (bf16[256,2048]{1,0:T(8,128)(2,1)S(1)}, bf16[256,2048]{1,0:T(8,128)(2,1)S(1)}, u32[]{:S(2)}, u32[]{:S(2)}) collective-permute-start(bf16[256,2048]{1,0:T(8,128)(2,1)S(1)} %fusion.1), channel_id=1, source_target_pairs={{0,30},{1,3},{2,0},{3,5},{4,2},{5,7},{6,4},{7,9},{8,6},{9,11},{10,... | collective-permute-start | bytes 3145736 | tf_op jit(solution)/shard_map/ppermute | solution.py:225
  289.4 22.0 %collective-permute-start.40 = (bf16[256,2048]{1,0:T(8,128)(2,1)S(1)}, bf16[256,2048]{1,0:T(8,128)(2,1)S(1)}, u32[]{:S(2)}, u32[]{:S(2)}) collective-permute-start(bf16[256,2048]{1,0:T(8,128)(2,1)S(1)} %fusion.4), channel_id=1, source_target_pairs={{0,30},{1,3},{2,0},{3,5},{4,2},{5,7},{6,4},{7,9},{8,6},{9,11},{10,... | collective-permute-start | bytes 3145736 | tf_op jit(solution)/shard_map/ppermute | solution.py:225
  300.6 22.0 %collective-permute-start.32 = (bf16[256,2048]{1,0:T(8,128)(2,1)S(1)}, bf16[256,2048]{1,0:T(8,128)(2,1)S(1)}, u32[]{:S(2)}, u32[]{:S(2)}) collective-permute-start(bf16[256,2048]{1,0:T(8,128)(2,1)S(1)} %fusion), channel_id=1, source_target_pairs={{0,30},{1,3},{2,0},{3,5},{4,2},{5,7},{6,4},{7,9},{8,6},{9,11},{10,... | collective-permute-start | bytes 3145736 | tf_op jit(solution)/shard_map/ppermute | solution.py:225
  311.4 11.2 %collective-permute-start.41 = (bf16[256,2048]{1,0:T(8,128)(2,1)S(1)}, bf16[256,2048]{1,0:T(8,128)(2,1)S(1)}, u32[]{:S(2)}, u32[]{:S(2)}) collective-permute-start(bf16[256,2048]{1,0:T(8,128)(2,1)S(1)} %collective-permute-done.40), channel_id=1, source_target_pairs={{0,1},{1,0},{2,3},{3,2},{4,5},{5,4},{6,7},{7,6},{8,9},{9,8},{10,11... | collective-permute-start | bytes 3145736 | tf_op jit(solution)/shard_map/ppermute | solution.py:232
  (14 other events, 73.5 us)
